TPU v7x, 128 devices: a whole 4x4x4 slice. The times are simulated.
128 devices in a mesh: fs: 16 (over z, x), tp: 8 (over y, core).
Axes of the slice: x: 4, y: 4, z: 4, core: 2. Of those that a mesh axis runs over, the one named last changes fastest.
Arguments:
- normed_input: bfloat16 [32768, 2048], P('fs'), may hold values from -6 to 6
- output_cotangent: bfloat16 [32768, 2048], P('fs'), may hold values from -6 to 6
- query_grad: bfloat16 [32768, 2048], P('fs', 'tp'), may hold values from -0.53033009 to 0.53033009
- key_grad: bfloat16 [32768, 2048], P('fs', 'tp'), may hold values from -0.53033009 to 0.53033009
- attn_values: bfloat16 [32768, 2048], P('fs', 'tp'), may hold values from -0.53033009 to 0.53033009
- master_weights: float32 [3, 2048, 2048], P(None, 'fs', 'tp'), may hold values from -3 to 3
- factors: bfloat16 [3, 2048, 256], P(None, 'fs'), may hold values from -0.375 to 0.375
- moments: float32 [3, 256, 2048], P(None, 'fs', 'tp'), may hold values from -620 to 620
Outputs:
- new_weights: float32 [3, 2048, 2048], P(None, 'fs', 'tp')
- weight_copies: bfloat16 [3, 2048, 2048], P(None, None, 'tp')
- steps: float32 [3, 2048, 2048], P(None, 'fs', 'tp')
- new_moments: float32 [3, 256, 2048], P(None, 'fs', 'tp')
All inputs are finite; a program needn't handle non-finite values.
Results may differ from a plain program's by a relative error of at most 0.0055.
Values may be sent and summed in bfloat16 or wider, within the bound.
No kernel may reach another device: no remote copies, remote signals or barrier semaphores. Data moves between devices by JAX's collectives and lax.ppermute only.
A program may use at most 128 MiB of HBM per device.

v0:
```python
import jax
import jax.numpy as jnp
from jax import lax
from jax.sharding import Mesh
from jax.sharding import PartitionSpec as P

FS = ("fs_0", "fs_1")
TP = ("tp_0", "tp_1")


def joined_along(blocks, dim):
    blocks = jnp.moveaxis(blocks, 0, dim)
    dims = blocks.shape
    return blocks.reshape(*dims[:dim], dims[dim] * dims[dim + 1], *dims[dim + 2 :])


def from_everyone(value, axis):
    copies = jnp.broadcast_to(value, (lax.axis_size(axis), *value.shape))
    return lax.all_to_all(copies, axis, split_axis=0, concat_axis=0, tiled=True)


def gathered_copies(value, axis, dim):
    return joined_along(from_everyone(value, axis), dim)


def in_blocks(value, dim, count):
    dims = value.shape
    blocks = value.reshape(*dims[:dim], count, dims[dim] // count, *dims[dim + 1 :])
    return jnp.moveaxis(blocks, dim, 0)


def sum_at_owner(value, axis, dim):
    count = lax.axis_size(axis)
    blocks = lax.all_to_all(in_blocks(value, dim, count), axis, 0, 0, tiled=True)
    return jnp.sum(blocks.astype(jnp.float32), axis=0)


def taken_together(value, axis):
    return from_everyone(value, axis).sum(axis=0)


def over_axes(value, axes):
    far, near = axes
    return taken_together(taken_together(value, near), far)


def on_device(
    normed_input,
    output_cotangent,
    query_grad,
    key_grad,
    attn_values,
    master_weights,
    factors,
    moments,
):
    rank_rows = moments.shape[1]
    width = query_grad.shape[1]
    rank = factors.shape[2]
    contract = (((0,), (0,)), ((), ()))
    whole_factors = gathered_copies(factors, FS, 1)
    reduced = [
        jnp.dot(normed_input, whole_factors[0], preferred_element_type=jnp.float32),
        jnp.dot(normed_input, whole_factors[1], preferred_element_type=jnp.float32),
        jnp.dot(output_cotangent, whole_factors[2], preferred_element_type=jnp.float32),
    ]
    head_sides = [query_grad, key_grad, attn_values]
    pieces = []
    for index in range(3):
        reduced_cols = reduced[index]
        pieces.append(
            lax.dot_general(
                reduced_cols,
                head_sides[index].astype(jnp.float32),
                contract,
                precision=lax.Precision.HIGHEST,
                preferred_element_type=jnp.float32,
            )
        )
    projected = sum_at_owner(jnp.concatenate(pieces, axis=1).astype(jnp.bfloat16), FS, 0)
    split = projected.reshape(rank_rows, 3, width).transpose(1, 0, 2)
    new_moments = 0.8 * moments + 0.2 * split
    total = over_axes(jnp.sum(new_moments * new_moments), (("fs_0", "fs_1", "tp_0"), "tp_1"))
    entries = 3 * rank * width * lax.axis_size(TP)
    rms = jnp.sqrt(total / entries + 1e-06)
    normalized = (new_moments / rms).astype(jnp.bfloat16)
    gathered = gathered_copies(normalized, FS, 1)
    steps = jnp.einsum("jdr,jrc->jdc", factors, gathered, preferred_element_type=jnp.float32)
    new_weights = master_weights - 0.05 * steps
    weight_copies = gathered_copies(new_weights.astype(jnp.bfloat16), FS, 1)
    return (new_weights, weight_copies, steps, new_moments)


def solution(mesh):
    split = Mesh(mesh.devices.reshape(4, 4, 4, 2), ("fs_0", "fs_1", "tp_0", "tp_1"))
    placed = (
        P(FS, None),
        P(FS, None),
        P(FS, TP),
        P(FS, TP),
        P(FS, TP),
        P(None, FS, TP),
        P(None, FS, None),
        P(None, FS, TP),
    )
    return jax.shard_map(
        on_device,
        mesh=split,
        in_specs=placed,
        out_specs=(P(None, FS, TP), P(None, None, TP), P(None, FS, TP), P(None, FS, TP)),
        check_vma=False,
    )
```

profile of v0, /device:TPU:0, one launch (start us, length us, event | category | flops | bytes accessed | tf_op | source)
XLA Modules:
  0.0 166.1 jit_solution(10673720153808837258)
XLA Ops:
  0.6 0.0 copy-start
  0.6 0.0 slice-start
  0.7 1.4 broadcast_in_dim.15
  2.1 0.0 slice-start.1
  2.1 47.7 %all_to_all.32 = bf16[16,3,128,256]{3,2,1,0:T(8,128)(2,1)S(1)} all-to-all(bf16[16,3,128,256]{3,2,1,0:T(8,128)(2,1)S(1)} %broadcast_in_dim.15), channel_id=1, replica_groups=mesh['fs_0'=4,'fs_1'=4,'tp_0'=4,'tp_1'=2] {'fs_0','fs_1'}, dimensions={0} | all-to-all | bytes 6291456 | tf_op jit(solution)/shard_map/all_to_all | solution.py:19
  49.8 0.2 fusion.1
  50.0 0.0 slice-done
  50.1 0.0 slice-done.1
  50.1 0.0 slice-start.2
  50.1 2.5 %fusion.2 = f32[2048,256]{1,0:T(8,128)S(1)} fusion(bf16[2048,2048]{1,0:T(8,128)(2,1)S(1)} %bitcast.42, bf16[2048,256]{1,0:T(8,128)(2,1)S(1)} %bitcast.37), kind=kOutput, calls=%fused_computation.14 | convolution fusion | flops 2147483648 | bytes 11534336 | tf_op jit(solution)/shard_map/dot_general | solution.py:63
  52.6 0.0 slice-start.3
  52.6 2.5 %fusion.3 = f32[2048,256]{1,0:T(8,128)S(1)} fusion(bf16[2048,2048]{1,0:T(8,128)(2,1)S(1)} %bitcast.42, bf16[2048,256]{1,0:T(8,128)(2,1)S(1)} %bitcast.36), kind=kOutput, calls=%fused_computation.15 | convolution fusion | flops 2147483648 | bytes 11534336 | tf_op jit(solution)/shard_map/dot_general | solution.py:64
  55.0 0.0 slice-done.2
  55.0 0.0 slice-done.3
  55.1 2.4 %fusion.4 = f32[2048,256]{1,0:T(8,128)S(1)} fusion(bf16[2048,2048]{1,0:T(8,128)(2,1)S(1)} %bitcast.44, bf16[2048,256]{1,0:T(8,128)(2,1)S(1)} %bitcast.35), kind=kOutput, calls=%fused_computation.16 | convolution fusion | flops 2147483648 | bytes 11534336 | tf_op jit(solution)/shard_map/dot_general | solution.py:65
  57.5 0.0 copy-done
  57.5 0.0 copy-start.1
  57.5 0.0 copy-start.2
  57.5 1.8 %convolution_convert_fusion = bf16[256,256]{1,0:T(8,128)(2,1)S(1)} fusion(f32[2048,256]{1,0:T(8,128)S(1)} %fusion.4, bf16[2048,256]{1,0:T(8,128)(2,1)S(1)} %copy-done), kind=kOutput, calls=%fused_computation.1 | convolution fusion | flops 1610678272 | bytes 3276800 | tf_op jit(solution)/shard_map/dot_general | solution.py:72
  59.4 0.0 copy-done.1
  59.4 1.8 %convolution_convert_fusion.2 = bf16[256,256]{1,0:T(8,128)(2,1)S(1)} fusion(f32[2048,256]{1,0:T(8,128)S(1)} %fusion.2, bf16[2048,256]{1,0:T(8,128)(2,1)S(1)} %copy-done.1), kind=kOutput, calls=%fused_computation.3 | convolution fusion | flops 1610678272 | bytes 3276800 | tf_op jit(solution)/shard_map/dot_general | solution.py:72
  61.2 0.0 copy-done.2
  61.2 0.0 copy-start.5
  61.3 0.0 copy-start.4
  61.3 2.0 %convolution_convert_fusion.1 = bf16[256,256]{1,0:T(8,128)(2,1)S(1)} fusion(f32[2048,256]{1,0:T(8,128)S(1)} %fusion.3, bf16[2048,256]{1,0:T(8,128)(2,1)S(1)} %copy-done.2), kind=kOutput, calls=%fused_computation.2 | convolution fusion | flops 1610678272 | bytes 3276800 | tf_op jit(solution)/shard_map/dot_general | solution.py:72
  63.3 0.0 copy-start.3
  63.3 12.5 %all_to_all.33 = bf16[16,16,768]{2,1,0:T(8,128)(2,1)S(1)} all-to-all(bf16[16,16,768]{2,1,0:T(8,128)(2,1)S(1)} %pad_maximum_fusion), channel_id=1, replica_groups=mesh['fs_0'=4,'fs_1'=4,'tp_0'=4,'tp_1'=2] {'fs_0','fs_1'}, dimensions={0} | all-to-all | bytes 786432 | tf_op jit(solution)/shard_map/all_to_all | solution.py:34
  75.8 0.1 convert_reduce_fusion
  75.9 0.7 multiply_reduce_fusion
  76.6 0.6 broadcast_in_dim.16
  77.2 3.7 %all_to_all.34 = f32[2,1,1]{2,1,0:T(1,128)S(1)} all-to-all(f32[2,1,1]{2,1,0:T(1,128)S(1)} %broadcast_in_dim.16), channel_id=1, replica_groups=mesh['fs_0'=4,'fs_1'=4,'tp_0'=4,'tp_1'=2] {'tp_1'}, dimensions={0} | all-to-all | bytes 16 | tf_op jit(solution)/shard_map/all_to_all | solution.py:19
  80.9 0.6 reduce_sum.38
  81.5 0.7 broadcast_in_dim.17
  82.2 16.0 %all_to_all.35 = f32[64,1,1]{2,1,0:T(1,128)S(1)} all-to-all(f32[64,1,1]{2,1,0:T(1,128)S(1)} %broadcast_in_dim.17), channel_id=1, replica_groups=mesh['fs_0'=4,'fs_1'=4,'tp_0'=4,'tp_1'=2] {'fs_0','fs_1','tp_0'}, dimensions={0} | all-to-all | bytes 512 | tf_op jit(solution)/shard_map/all_to_all | solution.py:19
  98.2 0.7 reduce_sum.39
  99.6 0.8 broadcast_in_dim.18
  100.4 3.6 %all-to-all-start.4 = ((bf16[16,3,16,256]{3,2,1,0:T(8,128)(2,1)}), bf16[16,3,16,256]{3,2,1,0:T(8,128)(2,1)S(1)}, u32[]{:S(2)}, u32[]{:S(2)}) async-start(bf16[16,3,16,256]{3,2,1,0:T(8,128)(2,1)} %broadcast_in_dim.18), calls=%async_computation.4 | async-start | bytes 786432 | tf_op jit(solution)/shard_map/all_to_all | solution.py:19
  104.0 0.2 copy.60
  104.1 9.2 %all-to-all-done.4 = bf16[16,3,16,256]{3,2,1,0:T(8,128)(2,1)S(1)} async-done(((bf16[16,3,16,256]{3,2,1,0:T(8,128)(2,1)}), bf16[16,3,16,256]{3,2,1,0:T(8,128)(2,1)S(1)}, u32[]{:S(2)}, u32[]{:S(2)}) %all-to-all-start.4) | async-done | bytes 393248 | tf_op jit(solution)/shard_map/all_to_all | solution.py:19
  113.4 0.3 fusion
  113.7 0.1 copy.61
  113.8 2.0 %broadcast_in_dim.19 = bf16[16,3,128,256]{3,2,1,0:T(8,128)(2,1)} broadcast(bf16[3,128,256]{2,1,0:T(8,128)(2,1)S(1)} %copy.61), dimensions={1,2,3} | broadcast | bytes 3342336 | tf_op jit(solution)/shard_map/broadcast_in_dim | solution.py:18
  115.9 4.5 %all-to-all-start.5 = ((bf16[16,3,128,256]{3,2,1,0:T(8,128)(2,1)}), bf16[16,3,128,256]{3,2,1,0:T(8,128)(2,1)}, u32[]{:S(2)}, u32[]{:S(2)}) async-start(bf16[16,3,128,256]{3,2,1,0:T(8,128)(2,1)} %broadcast_in_dim.19), calls=%async_computation.5 | async-start | bytes 6291456 | tf_op jit(solution)/shard_map/all_to_all | solution.py:19
  120.4 0.6 copy.65
  121.0 0.9 copy.63
  121.9 0.9 copy.64
  122.8 39.4 %all-to-all-done.5 = bf16[16,3,128,256]{3,2,1,0:T(8,128)(2,1)} async-done(((bf16[16,3,128,256]{3,2,1,0:T(8,128)(2,1)}), bf16[16,3,128,256]{3,2,1,0:T(8,128)(2,1)}, u32[]{:S(2)}, u32[]{:S(2)}) %all-to-all-start.5) | async-done | bytes 3145760 | tf_op jit(solution)/shard_map/all_to_all | solution.py:19
  162.2 3.9 %copy.62 = bf16[16,3,128,256]{3,2,0,1:T(8,128)(2,1)} copy(bf16[16,3,128,256]{3,2,1,0:T(8,128)(2,1)} %all-to-all-done.5) | data formatting | bytes 6291456 | tf_op jit(solution)/shard_map/all_to_all | solution.py:19
  (11 shorter events, 0.1 us)
Async XLA Ops:
  0.6 56.9 %copy-start = (bf16[2048,256]{1,0:T(8,128)(2,1)S(1)}, bf16[2048,256]{1,0:T(8,128)(2,1)}, u32[]{:S(2)}) copy-start(bf16[2048,256]{1,0:T(8,128)(2,1)} %param.12) | copy-start | bytes 3145732
  0.6 49.4 %slice-start = ((s8[8388608]{0:T(1024)(128)(4,1)}), s8[4194304]{0:T(1024)(128)(4,1)S(1)}, s32[]{:S(2)}) async-start(s8[8388608]{0:T(1024)(128)(4,1)} %bitcast.41), calls=%async_computation.6 | async-start | bytes 8388608
  2.1 48.0 %slice-start.1 = ((s8[8388608]{0:T(1024)(128)(4,1)}), s8[4194304]{0:T(1024)(128)(4,1)S(1)}, s32[]{:S(2)}) async-start(s8[8388608]{0:T(1024)(128)(4,1)} %bitcast.41), calls=%async_computation.7 | async-start | bytes 8388608
  50.1 5.0 %slice-start.2 = ((s8[8388608]{0:T(1024)(128)(4,1)}), s8[4194304]{0:T(1024)(128)(4,1)S(1)}, s32[]{:S(2)}) async-start(s8[8388608]{0:T(1024)(128)(4,1)} %bitcast.43), calls=%async_computation.8 | async-start | bytes 8388608
  52.6 2.5 %slice-start.3 = ((s8[8388608]{0:T(1024)(128)(4,1)}), s8[4194304]{0:T(1024)(128)(4,1)S(1)}, s32[]{:S(2)}) async-start(s8[8388608]{0:T(1024)(128)(4,1)} %bitcast.43), calls=%async_computation.9 | async-start | bytes 8388608
  57.5 1.9 %copy-start.1 = (bf16[2048,256]{1,0:T(8,128)(2,1)S(1)}, bf16[2048,256]{1,0:T(8,128)(2,1)}, u32[]{:S(2)}) copy-start(bf16[2048,256]{1,0:T(8,128)(2,1)} %param.10) | copy-start | bytes 3145732
  57.5 3.7 %copy-start.2 = (bf16[2048,256]{1,0:T(8,128)(2,1)S(1)}, bf16[2048,256]{1,0:T(8,128)(2,1)}, u32[]{:S(2)}) copy-start(bf16[2048,256]{1,0:T(8,128)(2,1)} %param.11) | copy-start | bytes 3145732
  61.2 14.7 %copy-start.5 = (f32[3,16,256]{2,1,0:T(8,128)S(1)}, f32[3,16,256]{2,1,0:T(8,128)}, u32[]{:S(2)}) copy-start(f32[3,16,256]{2,1,0:T(8,128)} %param.15) | copy-start | bytes 147460
  61.3 42.7 %copy-start.4 = (f32[3,128,256]{2,1,0:T(8,128)S(1)}, f32[3,128,256]{2,1,0:T(8,128)}, u32[]{:S(2)}) copy-start(f32[3,128,256]{2,1,0:T(8,128)} %param.13) | copy-start | bytes 1179652
  63.3 50.1 %copy-start.3 = (bf16[3,128,256]{2,1,0:T(8,128)(2,1)S(1)}, bf16[3,128,256]{2,1,0:T(8,128)(2,1)}, u32[]{:S(2)}) copy-start(bf16[3,128,256]{2,1,0:T(8,128)(2,1)} %param.14) | copy-start | bytes 589828
  100.4 12.9 %all-to-all-start.4 = ((bf16[16,3,16,256]{3,2,1,0:T(8,128)(2,1)}), bf16[16,3,16,256]{3,2,1,0:T(8,128)(2,1)S(1)}, u32[]{:S(2)}, u32[]{:S(2)}) async-start(bf16[16,3,16,256]{3,2,1,0:T(8,128)(2,1)} %broadcast_in_dim.18), calls=%async_computation.4 | async-start | bytes 786432 | tf_op jit(solution)/shard_map/all_to_all | solution.py:19
  115.9 46.3 %all-to-all-start.5 = ((bf16[16,3,128,256]{3,2,1,0:T(8,128)(2,1)}), bf16[16,3,128,256]{3,2,1,0:T(8,128)(2,1)}, u32[]{:S(2)}, u32[]{:S(2)}) async-start(bf16[16,3,128,256]{3,2,1,0:T(8,128)(2,1)} %broadcast_in_dim.19), calls=%async_computation.5 | async-start | bytes 6291456 | tf_op jit(solution)/shard_map/all_to_all | solution.py:19
where the time goes:
time: 167 us; the launch traced here: 166 us
  blocking collectives  79.9 us (48%)
  waiting for transfers between devices  48.6 us (29%)
  matrix products  13.4 us (8%)
  local copies, waits for them, and re-layouts  12.6 us (8%)
  starting transfers between devices  8.03 us (5%)
  other arithmetic  2.04 us (1%)
    all_to_all x3, blocking collectives, from_everyone(): return lax.all_to_all(copies, axis, split_axis=0, concat_axis=0, tiled=True)  67.4 us
    all_to_all x2, waiting for transfers between devices, from_everyone(): return lax.all_to_all(copies, axis, split_axis=0, concat_axis=0, tiled=True)  48.6 us
    all_to_all x1, blocking collectives, sum_at_owner(): lax.all_to_all(in_blocks(value, dim, count), axis, 0, 0, tiled=True)  12.5 us
    all_to_all x2, starting transfers between devices, from_everyone(): return lax.all_to_all(copies, axis, split_axis=0, concat_axis=0, tiled=True)  8.03 us
    dot_general x3, matrix products, on_device(): lax.dot_general(reduced_cols, head_sides[index].astype(jnp.float32), cont...  5.69 us
    broadcast_in_dim x5, local copies, waits for them, and re-layouts, from_everyone(): copies = jnp.broadcast_to(value, (lax.axis_size(axis), *value.shape))  5.56 us
    all_to_all x2, local copies, waits for them, and re-layouts, from_everyone(): return lax.all_to_all(copies, axis, split_axis=0, concat_axis=0, tiled=True)  3.93 us
  transfers between devices with their start and end apart: 2, of which 2 were waited for; matrix products, arithmetic and copies ran while one was open for 2% of the time, Pallas kernels for 0%

commit v1 on v0

v1 whole, which is shorter than its diff:
```python
import jax
import jax.numpy as jnp
from jax import lax
from jax.experimental import pallas as pl
from jax.experimental.pallas import tpu as pltpu
from jax.sharding import Mesh
from jax.sharding import PartitionSpec as P


Z, X, Y, C = "fs_0", "fs_1", "tp_0", "tp_1"
FS = (Z, X)
TP = (Y, C)
BF = jnp.bfloat16
F32 = jnp.float32


def swap(value):
    return lax.ppermute(value, C, [(0, 1), (1, 0)])


def turn(value, first, by):
    pairs = []
    for z in range(4):
        for x in range(4):
            for y in range(4):
                for c in range(2):
                    along_x = (c == 0) == first
                    to_z, to_x = (z, (x + by) % 4) if along_x else ((z + by) % 4, x)
                    pairs.append((((z * 4 + x) * 4 + y) * 2 + c, ((to_z * 4 + to_x) * 4 + y) * 2 + c))
    return lax.ppermute(value, FS + TP, pairs)


def exchange(value, axes):
    return lax.all_to_all(value, axes, 0, 0, tiled=True)


def vmem(count):
    return [pl.BlockSpec(memory_space=pltpu.VMEM) for _ in range(count)]


def hbm(count):
    return [pl.BlockSpec(memory_space=pltpu.HBM) for _ in range(count)]


def call(kernel, outs, args, scratch=(), mib=16, ins=None, out_specs=None):
    return pl.pallas_call(
        kernel,
        out_shape=outs,
        in_specs=ins or vmem(len(args)),
        out_specs=out_specs or vmem(len(outs)),
        scratch_shapes=list(scratch),
        compiler_params=pltpu.CompilerParams(vmem_limit_bytes=mib * 1024 * 1024),
    )(*args)


def behind(index, by):
    return lax.rem(index - by + 4, 4)


def after(value, *others):
    return lax.optimization_barrier((value, *others))[0]


def spread_kernel(factors, out):
    row = pl.multiple_of(lax.axis_index(C) * 64, 64)
    half = factors[:, pl.ds(row, 64), :]
    for f in range(16):
        out[f] = half


def gradient_kernel(first, second, q, k, v, out, a, b, sides, turned, acc, a_sems, b_sems, side_sems):
    halves = [pl.ds(0, 1024), pl.ds(1024, 1024)]
    side_loads = [pltpu.make_async_copy(r, sides.at[j], side_sems.at[j]) for j, r in enumerate((q, k, v))]
    a_loads = [pltpu.make_async_copy(first.at[h], a.at[h], a_sems.at[i]) for i, h in enumerate(halves)]
    b_loads = [pltpu.make_async_copy(second.at[h], b.at[h], b_sems.at[i]) for i, h in enumerate(halves)]
    for load in side_loads[:2] + a_loads[:1] + side_loads[2:] + a_loads[1:] + b_loads:
        load.start()
    for j in range(2):
        side_loads[j].wait()
        turned[256 * j : 256 * j + 256, :] = sides[j].T
    a_loads[0].wait()

    @pl.loop(0, 8)
    def _(i):
        cols = pl.ds(pl.multiple_of(i * 256, 256), 256)
        acc[:, cols] = jnp.dot(turned[0:512, 0:1024], a[0:1024, cols], preferred_element_type=F32)

    side_loads[2].wait()
    turned[512:768, :] = sides[2].T
    a_loads[1].wait()

    @pl.loop(0, 8)
    def _(i):
        cols = pl.ds(pl.multiple_of(i * 256, 256), 256)
        found = acc[:, cols] + jnp.dot(turned[0:512, 1024:2048], a[1024:2048, cols], preferred_element_type=F32)
        out[0, :, cols] = found[0:256].astype(BF)
        out[1, :, cols] = found[256:512].astype(BF)

    for load in b_loads:
        load.wait()

    @pl.loop(0, 8)
    def _(i):
        cols = pl.ds(pl.multiple_of(i * 256, 256), 256)
        out[2, :, cols] = jnp.dot(turned[512:768, :], b[:, cols], preferred_element_type=F32).astype(BF)


def gradients(*args):
    (out,) = call(
        gradient_kernel,
        [jax.ShapeDtypeStruct((3, 256, 2048), BF)],
        args,
        [
            pltpu.VMEM((2048, 2048), BF),
            pltpu.VMEM((2048, 2048), BF),
            pltpu.VMEM((3, 2048, 256), BF),
            pltpu.VMEM((768, 2048), BF),
            pltpu.VMEM((512, 2048), F32),
            pltpu.SemaphoreType.DMA((2,)),
            pltpu.SemaphoreType.DMA((2,)),
            pltpu.SemaphoreType.DMA((3,)),
        ],
        mib=58,
        ins=hbm(5),
    )
    return out


def project_kernel(mine, mate, grads, parts, whole):
    core = lax.axis_index(C)
    here = pl.multiple_of(core * 64, 64)
    there = pl.multiple_of((1 - core) * 64, 64)
    for f in range(16):
        for j in range(3):
            whole[j, pl.ds(f * 128 + here, 64), :] = mine[f, j]
            whole[j, pl.ds(f * 128 + there, 64), :] = mate[f, j]
    for j in range(3):
        total = jnp.dot(grads[j], whole[j], preferred_element_type=F32).T
        for f in range(16):
            parts[f, j] = total[16 * f : 16 * f + 16, :].astype(BF)


def moment_kernel(parts, moments, spread, new_moments):
    for j in range(3):
        s = parts[0, j].astype(F32)
        for f in range(1, 16):
            s = s + parts[f, j].astype(F32)
        m = 0.8 * moments[j] + 0.2 * s
        new_moments[j] = m
        rounded = m.astype(BF)
        for f in range(16):
            spread[f, j] = rounded


def join_kernel(gathered, joined, squares):
    acc = jnp.zeros((16, 256), F32)
    for j in range(3):
        for f in range(16):
            block = gathered[f, j]
            joined[j, 16 * f : 16 * f + 16, :] = block
            wide = block.astype(F32)
            acc = acc + wide * wide
    squares[...] = jnp.broadcast_to(jnp.sum(acc, axis=(0, 1), keepdims=True).reshape(1, 1, 1), squares.shape)


def back_kernel(joined, factors, mine, mate, found, own, whole, made, own_sems, mate_sems, out_sems):
    core = lax.axis_index(C)
    here = pl.multiple_of(core * 64, 64)
    there = pl.multiple_of((1 - core) * 64, 64)
    pairs = []
    for f in range(16):
        pairs.append(
            (
                pltpu.make_async_copy(mine.at[f], whole.at[:, pl.ds(f * 128 + here, 64), :], own_sems.at[f]),
                pltpu.make_async_copy(mate.at[f], whole.at[:, pl.ds(f * 128 + there, 64), :], mate_sems.at[f]),
            )
        )
    for a, b in pairs:
        a.start()
        b.start()
    for j in range(3):
        own[j] = jnp.dot(factors[j], joined[j], preferred_element_type=F32)
    stores = []
    for chunk in range(4):
        for a, b in pairs[4 * chunk : 4 * chunk + 4]:
            a.wait()
            b.wait()
        rows = pl.ds(512 * chunk, 512)
        for j in range(3):
            made[j, rows, :] = jnp.dot(whole[j, rows, :], joined[j], preferred_element_type=F32).astype(BF)
        store = pltpu.make_async_copy(made.at[:, rows, :], found.at[:, rows, :], out_sems.at[chunk])
        store.start()
        stores.append(store)
    for store in stores:
        store.wait()


def update_kernel(entries, squares, found, own, master, line, back, low, high, front, *refs):
    new_weights, steps, copies = refs[0:3]
    blocks, backs, made, block_sems, back_sems, out_sems = refs[3:9]
    z, x, core = lax.axis_index(Z), lax.axis_index(X), lax.axis_index(C)
    loads = []
    count = 0
    for far, source, nears in (
        (0, line, (0, 1, 2, 3)),
        (1, back, (0, 1, 2, 3)),
        (2, low, (0, 1)),
        (2, high, (2, 3)),
        (3, front, (0, 1, 2, 3)),
    ):
        for near in nears:
            owner = jnp.where(
                core == 0,
                behind(z, far) * 4 + behind(x, near),
                behind(z, near) * 4 + behind(x, far),
            )
            row = pl.multiple_of(owner * 128, 128)
            loads.append(
                pltpu.make_async_copy(
                    source.at[near - nears[0]], blocks.at[:, pl.ds(row, 128), :], block_sems.at[count]
                )
            )
            count += 1
    for load in loads:
        load.start()
    fills = []
    for chunk in range(4):
        rows = pl.ds(512 * chunk, 512)
        fill = pltpu.make_async_copy(found.at[:, rows, :], backs.at[:, rows, :], back_sems.at[chunk])
        fill.start()
        fills.append(fill)
    sums = jnp.sum(squares[...], axis=(0, 1))
    inverse = lax.rsqrt(sums.reshape(1, 128)[0:1, 0:1] / entries + 1e-06)
    scale = 0.05 * inverse
    for j in range(3):
        step = own[j] * inverse
        steps[j] = step
        new_weights[j] = master[j] - 0.05 * step
    for load in loads:
        load.wait()
    stores = []
    for chunk in range(4):
        rows = pl.ds(512 * chunk, 512)
        fills[chunk].wait()
        for j in range(3):
            made[j, rows, :] = (blocks[j, rows, :].astype(F32) - scale * backs[j, rows, :].astype(F32)).astype(BF)
        store = pltpu.make_async_copy(made.at[:, rows, :], copies.at[:, rows, :], out_sems.at[chunk])
        store.start()
        stores.append(store)
    for store in stores:
        store.wait()


def on_device(
    normed_input,
    output_cotangent,
    query_grad,
    key_grad,
    attn_values,
    master_weights,
    factors,
    moments,
):
    (spread,) = call(spread_kernel, [jax.ShapeDtypeStruct((16, 3, 64, 256), BF)], [factors])
    mine = exchange(spread, FS)

    own = master_weights.astype(BF)
    near_back = turn(own, True, 1)
    near_front = turn(own, True, -1)
    grads = gradients(normed_input, output_cotangent, query_grad, key_grad, attn_values)
    mine = after(mine, grads)
    mate = swap(mine)
    near_low = turn(after(near_back, mine)[:, :64], True, 1)
    near_high = turn(after(near_front, mine)[:, 64:], True, -1)
    line = jnp.stack([own, near_back, jnp.concatenate([near_low, near_high], axis=1), near_front])

    back = turn(line, False, 1)
    front = turn(line, False, -1)

    (parts,) = call(
        project_kernel,
        [jax.ShapeDtypeStruct((16, 3, 16, 256), BF)],
        [mine, mate, grads],
        [pltpu.VMEM((3, 2048, 256), BF)],
    )
    received = exchange(parts, FS)
    normal, new_moments = call(
        moment_kernel,
        [jax.ShapeDtypeStruct((16, 3, 16, 256), BF), jax.ShapeDtypeStruct((3, 16, 256), F32)],
        [received, moments],
    )
    gathered = exchange(normal, FS)
    joined, squares = call(
        join_kernel,
        [jax.ShapeDtypeStruct((3, 256, 256), BF), jax.ShapeDtypeStruct((8, 1, 128), F32)],
        [gathered],
    )
    all_squares = exchange(squares, TP)
    low = turn(back[:2], False, 1)
    high = turn(front[2:], False, -1)

    entries = 3 * 256 * 2048
    shard = jax.ShapeDtypeStruct((3, 128, 256), F32)
    found, own_found = call(
        back_kernel,
        [jax.ShapeDtypeStruct((3, 2048, 256), BF), shard],
        [joined, factors, mine, mate],
        [
            pltpu.VMEM((3, 2048, 256), BF),
            pltpu.VMEM((3, 2048, 256), BF),
            pltpu.SemaphoreType.DMA((16,)),
            pltpu.SemaphoreType.DMA((16,)),
            pltpu.SemaphoreType.DMA((4,)),
        ],
        mib=58,
        ins=vmem(2) + hbm(2),
        out_specs=hbm(1) + vmem(1),
    )
    new_weights, steps, weight_copies = call(
        lambda *refs: update_kernel(entries, *refs),
        [shard, shard, jax.ShapeDtypeStruct((3, 2048, 256), BF)],
        [all_squares, found, own_found, master_weights, line, back, low, high, front],
        [
            pltpu.VMEM((3, 2048, 256), BF),
            pltpu.VMEM((3, 2048, 256), BF),
            pltpu.VMEM((3, 2048, 256), BF),
            pltpu.SemaphoreType.DMA((16,)),
            pltpu.SemaphoreType.DMA((4,)),
            pltpu.SemaphoreType.DMA((4,)),
        ],
        mib=58,
        ins=vmem(1) + hbm(1) + vmem(2) + hbm(5),
        out_specs=vmem(2) + hbm(1),
    )
    return (new_weights, weight_copies, steps, new_moments)


def solution(mesh):
    split = Mesh(mesh.devices.reshape(4, 4, 4, 2), (Z, X, Y, C))
    placed = (
        P(FS, None),
        P(FS, None),
        P(FS, TP),
        P(FS, TP),
        P(FS, TP),
        P(None, FS, TP),
        P(None, FS, None),
        P(None, FS, TP),
    )

    return jax.shard_map(
        on_device,
        mesh=split,
        in_specs=placed,
        out_specs=(P(None, FS, TP), P(None, None, TP), P(None, FS, TP), P(None, FS, TP)),
        check_vma=False,
    )
```

time: 167 us -> 106 us (0.63)
  blocking collectives: 79.9 us -> 14.4 us
  Pallas kernels: 0 us -> 33.6 us
  waiting for transfers between devices: 48.6 us -> 24 us
  starting transfers between devices: 8.03 us -> 25.9 us
  matrix products: 13.4 us -> 0 us
  local copies, waits for them, and re-layouts: 12.6 us -> 4.59 us
    all_to_all x4 -> x1, blocking collectives: 79.9 us -> 14.4 us  [exchange(): return lax.all_to_all(value, axes, 0, 0, tiled=True)]
    all_to_all x2 -> x3, waiting for transfers between devices: 48.6 us -> 9.08 us  [exchange(): return lax.all_to_all(value, axes, 0, 0, tiled=True)]
    pallas_call x0 -> x7, Pallas kernels: none -> 33.6 us  [call(): pl.pallas_call(kernel, out_shape=outs, in_specs=ins or vmem(len(args)), o...]
    ppermute x0 -> x9, waiting for transfers between devices: none -> 15 us  [the longest x8 15 us: turn(): return lax.ppermute(value, FS + TP, pairs)]
    dot_general x7 -> x0, matrix products: 13.4 us -> none  [the longest x3 5.69 us: on_device(): lax.dot_general(reduced_cols, head_sides[index].astype(jnp.float32), cont...]
    all_to_all x2 -> x3, starting transfers between devices: 8.03 us -> 17.2 us  [exchange(): return lax.all_to_all(value, axes, 0, 0, tiled=True)]
    ppermute x0 -> x9, starting transfers between devices: none -> 8.71 us  [the longest x8 8.7 us: turn(): return lax.ppermute(value, FS + TP, pairs)]
    broadcast_in_dim x5 -> x0, local copies, waits for them, and re-layouts: 5.56 us -> none  [from_everyone(): copies = jnp.broadcast_to(value, (lax.axis_size(axis), *value.shape))]
  transfers between devices with their start and end apart: 2 -> 12, of which waited for: 2 -> 8; matrix products, arithmetic and copies ran while one was open for 2% -> 3% of each run, Pallas kernels for 0% -> 24%
where the time goes in v1:
time: 106 us; the launch traced here: 104 us
  Pallas kernels  33.6 us (32%)
  starting transfers between devices  25.9 us (24%)
  waiting for transfers between devices  24 us (23%)
  blocking collectives  14.4 us (14%)
  local copies, waits for them, and re-layouts  4.59 us (4%)
  other arithmetic  1.08 us (1%)
    pallas_call x7, Pallas kernels, call(): pl.pallas_call(kernel, out_shape=outs, in_specs=ins or vmem(len(args)), o...  33.6 us
    all_to_all x3, starting transfers between devices, exchange(): return lax.all_to_all(value, axes, 0, 0, tiled=True)  17.2 us
    ppermute x8, waiting for transfers between devices, turn(): return lax.ppermute(value, FS + TP, pairs)  15 us
    all_to_all x1, blocking collectives, exchange(): return lax.all_to_all(value, axes, 0, 0, tiled=True)  14.4 us
    all_to_all x3, waiting for transfers between devices, exchange(): return lax.all_to_all(value, axes, 0, 0, tiled=True)  9.08 us
    ppermute x8, starting transfers between devices, turn(): return lax.ppermute(value, FS + TP, pairs)  8.7 us
    unnamed x20, local copies, waits for them, and re-layouts  2.53 us
  transfers between devices with their start and end apart: 12, of which 8 were waited for; matrix products, arithmetic and copies ran while one was open for 3% of the time, Pallas kernels for 24%

profile of v1, /device:TPU:0, one launch (start us, length us, event | category | flops | bytes accessed | tf_op | source)
XLA Modules:
  0.0 104.3 jit_solution(3792109215717775232)
XLA Ops:
  0.6 0.0 copy-start.3
  0.6 0.9 copy-done.3
  1.6 1.3 %shard_map.111 = bf16[16,3,64,256]{3,2,1,0:T(8,128)(2,1)} custom-call(bf16[3,128,256]{2,1,0:T(8,128)(2,1)S(1)} %copy-done.3), custom_call_target="tpu_custom_call" | custom-call | tf_op jit(solution)/shard_map/pallas_call | solution.py:46
  2.9 8.0 %all-to-all-start = ((bf16[16,3,64,256]{3,2,1,0:T(8,128)(2,1)}), bf16[16,3,64,256]{3,2,1,0:T(8,128)(2,1)S(1)}, u32[]{:S(2)}, u32[]{:S(2)}) async-start(bf16[16,3,64,256]{3,2,1,0:T(8,128)(2,1)} %shard_map.111), calls=%async_computation | async-start | bytes 3145728 | tf_op jit(solution)/shard_map/all_to_all | solution.py:34
  10.9 0.0 copy-start.6
  10.9 15.9 %shard_map.112.grads = bf16[3,256,2048]{2,1,0:T(8,128)(2,1)} custom-call(bf16[2048,2048]{1,0:T(8,128)(2,1)} %first.1, bf16[2048,2048]{1,0:T(8,128)(2,1)} %second.1, bf16[2048,256]{1,0:T(8,128)(2,1)} %q.1, bf16[2048,256]{1,0:T(8,128)(2,1)} %k.1, bf16[2048,256]{1,0:T(8,128)(2,1)} %v.1), custom_call_target="tpu_custom_call" | custom-call | tf_op jit(solution)/shard_map/pallas_call | solution.py:46
  26.8 8.6 %all-to-all-done.mine = bf16[16,3,64,256]{3,2,1,0:T(8,128)(2,1)S(1)} async-done(((bf16[16,3,64,256]{3,2,1,0:T(8,128)(2,1)}), bf16[16,3,64,256]{3,2,1,0:T(8,128)(2,1)S(1)}, u32[]{:S(2)}, u32[]{:S(2)}) %all-to-all-start) | async-done | bytes 1572896 | tf_op jit(solution)/shard_map/all_to_all | solution.py:34
  35.4 0.0 collective-permute-start
  35.4 0.0 copy-done.6
  35.5 0.1 collective-permute-start.3
  35.5 2.0 %collective-permute-start.1 = (bf16[3,128,256]{2,1,0:T(8,128)(2,1)S(1)}, bf16[3,128,256]{2,1,0:T(8,128)(2,1)S(1)}, u32[]{:S(2)}, u32[]{:S(2)}) collective-permute-start(bf16[3,128,256]{2,1,0:T(8,128)(2,1)S(1)} %convert_element_type.3), channel_id=1, source_target_pairs={{0,8},{1,33},{2,10},{3,35},{4,12},{5,37},{6,14},{7,39},{8,16},{9,4... | collective-permute-start | bytes 589832 | tf_op jit(solution)/shard_map/ppermute | solution.py:30
  37.5 3.6 %collective-permute-done.3 = bf16[3,128,256]{2,1,0:T(8,128)(2,1)S(1)} collective-permute-done((bf16[3,128,256]{2,1,0:T(8,128)(2,1)S(1)}, bf16[3,128,256]{2,1,0:T(8,128)(2,1)S(1)}, u32[]{:S(2)}, u32[]{:S(2)}) %collective-permute-start.3) | collective-permute-done | bytes 196640 | tf_op jit(solution)/shard_map/ppermute | solution.py:30
  41.2 1.3 %collective-permute-done.1 = bf16[3,128,256]{2,1,0:T(8,128)(2,1)S(1)} collective-permute-done((bf16[3,128,256]{2,1,0:T(8,128)(2,1)S(1)}, bf16[3,128,256]{2,1,0:T(8,128)(2,1)S(1)}, u32[]{:S(2)}, u32[]{:S(2)}) %collective-permute-start.1) | collective-permute-done | bytes 196640 | tf_op jit(solution)/shard_map/ppermute | solution.py:30
  42.5 0.1 collective-permute-start.4
  42.6 2.0 %collective-permute-start.2 = (bf16[3,64,256]{2,1,0:T(8,128)(2,1)S(1)}, bf16[3,64,256]{2,1,0:T(8,128)(2,1)S(1)}, u32[]{:S(2)}, u32[]{:S(2)}) collective-permute-start(bf16[3,64,256]{2,1,0:T(8,128)(2,1)S(1)} %slice.12), channel_id=1, source_target_pairs={{0,8},{1,33},{2,10},{3,35},{4,12},{5,37},{6,14},{7,39},{8,16},{9,4... | collective-permute-start | bytes 294920 | tf_op jit(solution)/shard_map/ppermute | solution.py:30
  44.6 2.6 %collective-permute-done.4 = bf16[3,64,256]{2,1,0:T(8,128)(2,1)S(1)} collective-permute-done((bf16[3,64,256]{2,1,0:T(8,128)(2,1)S(1)}, bf16[3,64,256]{2,1,0:T(8,128)(2,1)S(1)}, u32[]{:S(2)}, u32[]{:S(2)}) %collective-permute-start.4) | collective-permute-done | bytes 98336 | tf_op jit(solution)/shard_map/ppermute | solution.py:30
  47.2 1.3 %collective-permute-done.2 = bf16[3,64,256]{2,1,0:T(8,128)(2,1)S(1)} collective-permute-done((bf16[3,64,256]{2,1,0:T(8,128)(2,1)S(1)}, bf16[3,64,256]{2,1,0:T(8,128)(2,1)S(1)}, u32[]{:S(2)}, u32[]{:S(2)}) %collective-permute-start.2) | collective-permute-done | bytes 98336 | tf_op jit(solution)/shard_map/ppermute | solution.py:30
  48.5 1.0 pad_maximum_fusion.refs_4_
  49.5 1.1 %collective-permute-start.7 = (bf16[4,3,128,256]{3,2,1,0:T(8,128)(2,1)}, bf16[4,3,128,256]{3,2,1,0:T(8,128)(2,1)}, u32[]{:S(2)}, u32[]{:S(2)}) collective-permute-start(bf16[4,3,128,256]{3,2,1,0:T(8,128)(2,1)} %pad_maximum_fusion.refs_4_), channel_id=1, source_target_pairs={{0,96},{1,25},{2,98},{3,27},{4,100},{5,29},{6,102},{7,31},{8,104},... | collective-permute-start | bytes 2359304 | tf_op jit(solution)/shard_map/ppermute | solution.py:30
  50.7 0.9 collective-permute-start.5
  51.6 0.0 collective-permute-done.mate
  51.6 0.0 copy-done.1
  51.6 2.0 %shard_map.113 = bf16[16,3,16,256]{3,2,1,0:T(8,128)(2,1)} custom-call(bf16[16,3,64,256]{3,2,1,0:T(8,128)(2,1)S(1)} %all-to-all-done.mine, bf16[16,3,64,256]{3,2,1,0:T(8,128)(2,1)S(1)} %collective-permute-done.mate, bf16[3,256,2048]{2,1,0:T(8,128)(2,1)S(1)} %copy-done.1), custom_call_target="tpu_custom_call" | custom-call | tf_op jit(solution)/shard_map/pallas_call | solution.py:46
  53.6 0.0 copy-done
  53.6 0.0 copy-done.2
  53.6 4.7 %all-to-all-start.1 = ((bf16[16,3,16,256]{3,2,1,0:T(8,128)(2,1)}), bf16[16,3,16,256]{3,2,1,0:T(8,128)(2,1)S(1)}, u32[]{:S(2)}, u32[]{:S(2)}) async-start(bf16[16,3,16,256]{3,2,1,0:T(8,128)(2,1)} %shard_map.113), calls=%async_computation.1 | async-start | bytes 786432 | tf_op jit(solution)/shard_map/all_to_all | solution.py:34
  58.3 5.7 %collective-permute-done.7.refs_8_ = bf16[4,3,128,256]{3,2,1,0:T(8,128)(2,1)} collective-permute-done((bf16[4,3,128,256]{3,2,1,0:T(8,128)(2,1)}, bf16[4,3,128,256]{3,2,1,0:T(8,128)(2,1)}, u32[]{:S(2)}, u32[]{:S(2)}) %collective-permute-start.7) | collective-permute-done | bytes 786464 | tf_op jit(solution)/shard_map/ppermute | solution.py:30
  63.9 1.0 slice.17
  65.0 2.4 %collective-permute-start.8 = (bf16[2,3,128,256]{3,2,1,0:T(8,128)(2,1)S(1)}, bf16[2,3,128,256]{3,2,1,0:T(8,128)(2,1)S(1)}, u32[]{:S(2)}, u32[]{:S(2)}) collective-permute-start(bf16[2,3,128,256]{3,2,1,0:T(8,128)(2,1)S(1)} %slice.17), channel_id=1, source_target_pairs={{0,96},{1,25},{2,98},{3,27},{4,100},{5,29},{6,102},{7,31},{8,104},... | collective-permute-start | bytes 1179656 | tf_op jit(solution)/shard_map/ppermute | solution.py:30
  67.4 0.5 collective-permute-done.5.refs_5_
  67.9 1.0 slice.16
  68.9 0.1 collective-permute-start.6
  69.0 0.5 all-to-all-done.1.parts
  69.5 0.0 copy-done.5
  69.5 0.7 shard_map.114
  70.2 14.4 %all_to_all.20.gathered = bf16[16,3,16,256]{3,2,1,0:T(8,128)(2,1)S(1)} all-to-all(bf16[16,3,16,256]{3,2,1,0:T(8,128)(2,1)S(1)} %get-tuple-element.17), channel_id=1, replica_groups=mesh['fs_0'=4,'fs_1'=4,'tp_0'=4,'tp_1'=2] {'fs_0','fs_1'}, dimensions={0} | all-to-all | bytes 786432 | tf_op jit(solution)/shard_map/all_to_all | solution.py:34
  84.6 0.8 shard_map.115
  85.3 0.7 copy-done.4
  86.1 4.5 %all-to-all-start.3 = ((f32[8,1,128]{2,1,0:T(1,128)}), f32[8,1,128]{2,1,0:T(1,128)S(1)}, u32[]{:S(2)}, u32[]{:S(2)}) async-start(f32[8,1,128]{2,1,0:T(1,128)} %get-tuple-element.18), calls=%async_computation.3 | async-start | bytes 8192 | tf_op jit(solution)/shard_map/all_to_all | solution.py:34
  90.5 6.0 %shard_map.116 = (bf16[3,2048,256]{2,1,0:T(8,128)(2,1)}, f32[3,128,256]{2,1,0:T(8,128)}) custom-call(bf16[3,256,256]{2,1,0:T(8,128)(2,1)} %copy-done.4, bf16[3,128,256]{2,1,0:T(8,128)(2,1)} %factors.3, bf16[16,3,64,256]{3,2,1,0:T(8,128)(2,1)} %copy-done, bf16[16,3,64,256]{3,2,1,0:T(8,128)(2,1)} %copy-done.2), custom_call_target="tpu_custom_call" | custom-call | tf_op jit(solution)/shard_map/pallas_call | solution.py:46
  96.5 0.0 collective-permute-done.8.refs_7_
  96.5 0.0 copy-start.7
  96.5 0.0 collective-permute-done.6.refs_6_
  96.5 0.0 copy-start.8
  96.5 0.0 all-to-all-done.3.refs_0_
  96.6 0.7 copy-done.7
  97.3 0.1 copy-done.8
  97.4 6.9 %shard_map.117 = (f32[3,128,256]{2,1,0:T(8,128)}, f32[3,128,256]{2,1,0:T(8,128)}, bf16[3,2048,256]{2,1,0:T(8,128)(2,1)}) custom-call(f32[8,1,128]{2,1,0:T(1,128)} %copy-done.9, bf16[3,2048,256]{2,1,0:T(8,128)(2,1)} %get-tuple-element.20.refs_1_, f32[3,128,256]{2,1,0:T(8,128)} %get-tuple-element.21.refs_2_, f32[3,128,256]{2,1,0:T(8,128)} %refs_3_.1, ...), custom_call_target="tpu_custom_call" | custom-call | tf_op jit(solution)/shard_map/pallas_call | solution.py:46
  (12 shorter events, 0.1 us)
Async XLA Ops:
  0.6 0.9 copy-start.3
  2.9 32.5 %all-to-all-start = ((bf16[16,3,64,256]{3,2,1,0:T(8,128)(2,1)}), bf16[16,3,64,256]{3,2,1,0:T(8,128)(2,1)S(1)}, u32[]{:S(2)}, u32[]{:S(2)}) async-start(bf16[16,3,64,256]{3,2,1,0:T(8,128)(2,1)} %shard_map.111), calls=%async_computation | async-start | bytes 3145728 | tf_op jit(solution)/shard_map/all_to_all | solution.py:34
  10.9 24.5 %copy-start.6 = (f32[3,128,256]{2,1,0:T(8,128)S(1)}, f32[3,128,256]{2,1,0:T(8,128)}, u32[]{:S(2)}) copy-start(f32[3,128,256]{2,1,0:T(8,128)} %refs_3_.1) | copy-start | bytes 1179652
  35.4 18.2 %copy-start = (bf16[16,3,64,256]{3,2,1,0:T(8,128)(2,1)}, bf16[16,3,64,256]{3,2,1,0:T(8,128)(2,1)S(1)}, u32[]{:S(2)}) copy-start(bf16[16,3,64,256]{3,2,1,0:T(8,128)(2,1)S(1)} %all-to-all-done.mine) | copy-start | bytes 4718596
  35.4 16.2 %copy-start.1 = (bf16[3,256,2048]{2,1,0:T(8,128)(2,1)S(1)}, bf16[3,256,2048]{2,1,0:T(8,128)(2,1)}, u32[]{:S(2)}) copy-start(bf16[3,256,2048]{2,1,0:T(8,128)(2,1)} %shard_map.112.grads) | copy-start | bytes 9437188
  35.4 16.2 %collective-permute-start = (bf16[16,3,64,256]{3,2,1,0:T(8,128)(2,1)S(1)}, bf16[16,3,64,256]{3,2,1,0:T(8,128)(2,1)S(1)}, u32[]{:S(2)}, u32[]{:S(2)}) collective-permute-start(bf16[16,3,64,256]{3,2,1,0:T(8,128)(2,1)S(1)} %all-to-all-done.mine), channel_id=1, source_target_pairs={{0,1},{1,0},{2,3},{3,2},{4,5},{5,4},{6,7},{7,6},{8,9},{9,8},{10,11... | collective-permute-start | bytes 4718600 | tf_op jit(solution)/shard_map/ppermute | solution.py:18
  35.5 5.7 %collective-permute-start.3 = (bf16[3,128,256]{2,1,0:T(8,128)(2,1)S(1)}, bf16[3,128,256]{2,1,0:T(8,128)(2,1)S(1)}, u32[]{:S(2)}, u32[]{:S(2)}) collective-permute-start(bf16[3,128,256]{2,1,0:T(8,128)(2,1)S(1)} %convert_element_type.3), channel_id=1, source_target_pairs={{0,24},{1,97},{2,26},{3,99},{4,28},{5,101},{6,30},{7,103},{8,0},{9... | collective-permute-start | bytes 589832 | tf_op jit(solution)/shard_map/ppermute | solution.py:30
  35.5 6.9 %collective-permute-start.1 = (bf16[3,128,256]{2,1,0:T(8,128)(2,1)S(1)}, bf16[3,128,256]{2,1,0:T(8,128)(2,1)S(1)}, u32[]{:S(2)}, u32[]{:S(2)}) collective-permute-start(bf16[3,128,256]{2,1,0:T(8,128)(2,1)S(1)} %convert_element_type.3), channel_id=1, source_target_pairs={{0,8},{1,33},{2,10},{3,35},{4,12},{5,37},{6,14},{7,39},{8,16},{9,4... | collective-permute-start | bytes 589832 | tf_op jit(solution)/shard_map/ppermute | solution.py:30
  42.5 4.7 %collective-permute-start.4 = (bf16[3,64,256]{2,1,0:T(8,128)(2,1)S(1)}, bf16[3,64,256]{2,1,0:T(8,128)(2,1)S(1)}, u32[]{:S(2)}, u32[]{:S(2)}) collective-permute-start(bf16[3,64,256]{2,1,0:T(8,128)(2,1)S(1)} %slice.13), channel_id=1, source_target_pairs={{0,24},{1,97},{2,26},{3,99},{4,28},{5,101},{6,30},{7,103},{8,0},{9... | collective-permute-start | bytes 294920 | tf_op jit(solution)/shard_map/ppermute | solution.py:30
  42.6 5.9 %collective-permute-start.2 = (bf16[3,64,256]{2,1,0:T(8,128)(2,1)S(1)}, bf16[3,64,256]{2,1,0:T(8,128)(2,1)S(1)}, u32[]{:S(2)}, u32[]{:S(2)}) collective-permute-start(bf16[3,64,256]{2,1,0:T(8,128)(2,1)S(1)} %slice.12), channel_id=1, source_target_pairs={{0,8},{1,33},{2,10},{3,35},{4,12},{5,37},{6,14},{7,39},{8,16},{9,4... | collective-permute-start | bytes 294920 | tf_op jit(solution)/shard_map/ppermute | solution.py:30
  49.5 20.0 %copy-start.5 = (f32[3,16,256]{2,1,0:T(8,128)S(1)}, f32[3,16,256]{2,1,0:T(8,128)}, u32[]{:S(2)}) copy-start(f32[3,16,256]{2,1,0:T(8,128)} %moments.1) | copy-start | bytes 147460
  49.5 14.4 %collective-permute-start.7 = (bf16[4,3,128,256]{3,2,1,0:T(8,128)(2,1)}, bf16[4,3,128,256]{3,2,1,0:T(8,128)(2,1)}, u32[]{:S(2)}, u32[]{:S(2)}) collective-permute-start(bf16[4,3,128,256]{3,2,1,0:T(8,128)(2,1)} %pad_maximum_fusion.refs_4_), channel_id=1, source_target_pairs={{0,96},{1,25},{2,98},{3,27},{4,100},{5,29},{6,102},{7,31},{8,104},... | collective-permute-start | bytes 2359304 | tf_op jit(solution)/shard_map/ppermute | solution.py:30
  50.7 17.2 %collective-permute-start.5 = (bf16[4,3,128,256]{3,2,1,0:T(8,128)(2,1)}, bf16[4,3,128,256]{3,2,1,0:T(8,128)(2,1)}, u32[]{:S(2)}, u32[]{:S(2)}) collective-permute-start(bf16[4,3,128,256]{3,2,1,0:T(8,128)(2,1)} %pad_maximum_fusion.refs_4_), channel_id=1, source_target_pairs={{0,32},{1,9},{2,34},{3,11},{4,36},{5,13},{6,38},{7,15},{8,40},{9,1... | collective-permute-start | bytes 2359304 | tf_op jit(solution)/shard_map/ppermute | solution.py:30
  51.6 2.0 %copy-start.2 = (bf16[16,3,64,256]{3,2,1,0:T(8,128)(2,1)}, bf16[16,3,64,256]{3,2,1,0:T(8,128)(2,1)S(1)}, u32[]{:S(2)}) copy-start(bf16[16,3,64,256]{3,2,1,0:T(8,128)(2,1)S(1)} %collective-permute-done.mate) | copy-start | bytes 4718596
  53.6 15.9 %all-to-all-start.1 = ((bf16[16,3,16,256]{3,2,1,0:T(8,128)(2,1)}), bf16[16,3,16,256]{3,2,1,0:T(8,128)(2,1)S(1)}, u32[]{:S(2)}, u32[]{:S(2)}) async-start(bf16[16,3,16,256]{3,2,1,0:T(8,128)(2,1)} %shard_map.113), calls=%async_computation.1 | async-start | bytes 786432 | tf_op jit(solution)/shard_map/all_to_all | solution.py:34
  65.0 31.5 %collective-permute-start.8 = (bf16[2,3,128,256]{3,2,1,0:T(8,128)(2,1)S(1)}, bf16[2,3,128,256]{3,2,1,0:T(8,128)(2,1)S(1)}, u32[]{:S(2)}, u32[]{:S(2)}) collective-permute-start(bf16[2,3,128,256]{3,2,1,0:T(8,128)(2,1)S(1)} %slice.17), channel_id=1, source_target_pairs={{0,96},{1,25},{2,98},{3,27},{4,100},{5,29},{6,102},{7,31},{8,104},... | collective-permute-start | bytes 1179656 | tf_op jit(solution)/shard_map/ppermute | solution.py:30
  68.9 27.6 %collective-permute-start.6 = (bf16[2,3,128,256]{3,2,1,0:T(8,128)(2,1)S(1)}, bf16[2,3,128,256]{3,2,1,0:T(8,128)(2,1)S(1)}, u32[]{:S(2)}, u32[]{:S(2)}) collective-permute-start(bf16[2,3,128,256]{3,2,1,0:T(8,128)(2,1)S(1)} %slice.16), channel_id=1, source_target_pairs={{0,32},{1,9},{2,34},{3,11},{4,36},{5,13},{6,38},{7,15},{8,40},{9,1... | collective-permute-start | bytes 1179656 | tf_op jit(solution)/shard_map/ppermute | solution.py:30
  85.3 0.7 copy-start.4
  86.1 10.5 %all-to-all-start.3 = ((f32[8,1,128]{2,1,0:T(1,128)}), f32[8,1,128]{2,1,0:T(1,128)S(1)}, u32[]{:S(2)}, u32[]{:S(2)}) async-start(f32[8,1,128]{2,1,0:T(1,128)} %get-tuple-element.18), calls=%async_computation.3 | async-start | bytes 8192 | tf_op jit(solution)/shard_map/all_to_all | solution.py:34
  96.5 0.7 copy-start.7
  96.5 0.9 copy-start.8
  96.5 0.8 copy-start.9

commit v2 on v1

v2 whole, which is shorter than its diff:
```python
import jax
import jax.numpy as jnp
from jax import lax
from jax.experimental import pallas as pl
from jax.experimental.pallas import tpu as pltpu
from jax.sharding import Mesh
from jax.sharding import PartitionSpec as P


Z, X, Y, C = "fs_0", "fs_1", "tp_0", "tp_1"
FS = (Z, X)
TP = (Y, C)
BF = jnp.bfloat16
F32 = jnp.float32


def swap(value):
    return lax.ppermute(value, C, [(0, 1), (1, 0)])


def turn(value, first, by):
    pairs = []
    for z in range(4):
        for x in range(4):
            for y in range(4):
                for c in range(2):
                    along_x = (c == 0) == first
                    to_z, to_x = (z, (x + by) % 4) if along_x else ((z + by) % 4, x)
                    pairs.append((((z * 4 + x) * 4 + y) * 2 + c, ((to_z * 4 + to_x) * 4 + y) * 2 + c))
    return lax.ppermute(value, FS + TP, pairs)


def exchange(value, axes):
    return lax.all_to_all(value, axes, 0, 0, tiled=True)


def vmem(count):
    return [pl.BlockSpec(memory_space=pltpu.VMEM) for _ in range(count)]


def hbm(count):
    return [pl.BlockSpec(memory_space=pltpu.HBM) for _ in range(count)]


def call(kernel, outs, args, scratch=(), mib=16, ins=None, out_specs=None):
    return pl.pallas_call(
        kernel,
        out_shape=outs,
        in_specs=ins or vmem(len(args)),
        out_specs=out_specs or vmem(len(outs)),
        scratch_shapes=list(scratch),
        compiler_params=pltpu.CompilerParams(vmem_limit_bytes=mib * 1024 * 1024),
    )(*args)


def behind(index, by):
    return lax.rem(index - by + 4, 4)


def after(value, *others):
    return lax.optimization_barrier((value, *others))[0]


def spread_kernel(factors, out, half, sem, sems):
    row = pl.multiple_of(lax.axis_index(C) * 64, 64)
    load = pltpu.make_async_copy(factors.at[:, pl.ds(row, 64), :], half, sem)
    load.start()
    load.wait()
    moves = [pltpu.make_async_copy(half, out.at[f], sems.at[f]) for f in range(16)]
    for move in moves:
        move.start()
    for move in moves:
        move.wait()


def gradient_kernel(first, second, q, k, v, out, a, b, sides, left_sems, side_sems):
    for source, target, sem in (
        (q, sides.at[0], side_sems.at[0]),
        (k, sides.at[1], side_sems.at[1]),
        (first, a, left_sems.at[0]),
        (v, sides.at[2], side_sems.at[2]),
        (second, b, left_sems.at[1]),
    ):
        for i in range(8):
            rows = pl.ds(256 * i, 256)
            pltpu.make_async_copy(source.at[rows], target.at[rows], sem).start()
    for j, (side, left, block) in enumerate(((q, first, a), (k, first, a), (v, second, b))):
        pltpu.make_async_copy(side, sides.at[j], side_sems.at[j]).wait()
        if j != 1:
            pltpu.make_async_copy(left, block, left_sems.at[j // 2]).wait()
        out[j] = lax.dot_general(
            sides[j], block[...], (((0,), (0,)), ((), ())), preferred_element_type=F32
        ).astype(BF)


def held_in_hbm(values):
    return [pltpu.with_memory_space_constraint(v, pltpu.HBM) for v in values]


def gradients(*args):
    (out,) = call(
        gradient_kernel,
        [jax.ShapeDtypeStruct((3, 256, 2048), BF)],
        held_in_hbm(args),
        [
            pltpu.VMEM((2048, 2048), BF),
            pltpu.VMEM((2048, 2048), BF),
            pltpu.VMEM((3, 2048, 256), BF),
            pltpu.SemaphoreType.DMA((2,)),
            pltpu.SemaphoreType.DMA((3,)),
        ],
        mib=32,
        ins=hbm(5),
    )
    return out


def project_kernel(mine, mate, grads, parts, whole):
    core = lax.axis_index(C)
    here = pl.multiple_of(core * 64, 64)
    there = pl.multiple_of((1 - core) * 64, 64)
    for j in range(3):
        for f in range(16):
            whole[j, pl.ds(f * 128 + here, 64), :] = mine[f, j]
            whole[j, pl.ds(f * 128 + there, 64), :] = mate[f, j]
        total = jnp.dot(grads[j], whole[j], preferred_element_type=F32).T
        for f in range(16):
            parts[f, j] = total[16 * f : 16 * f + 16, :].astype(BF)


def moment_kernel(parts, held, spread, new_moments):
    for j in range(3):
        s = parts[0, j].astype(F32)
        for f in range(1, 16):
            s = s + parts[f, j].astype(F32)
        m = held[j] + 0.2 * s
        new_moments[j] = m
        rounded = m.astype(BF)
        for f in range(16):
            spread[f, j] = rounded


def join_kernel(gathered, squares):
    acc = jnp.zeros((16, 256), F32)
    for j in range(3):
        for f in range(16):
            wide = gathered[f, j].astype(F32)
            acc = acc + wide * wide
    squares[...] = jnp.broadcast_to(jnp.sum(acc, axis=(0, 1), keepdims=True).reshape(1, 1, 1), squares.shape)


def stack_kernel(own, back_top, back_bottom, low, high, front_top, front_bottom, moments, near, far, held):
    near[0] = own[...]
    near[1, :, 0:64, :] = back_top[...]
    near[1, :, 64:128, :] = back_bottom[...]
    far[0, :, 0:64, :] = low[...]
    far[0, :, 64:128, :] = high[...]
    far[1, :, 0:64, :] = front_top[...]
    far[1, :, 64:128, :] = front_bottom[...]
    held[...] = 0.8 * moments[...]


def update_kernel(entries, squares, gathered, far_first, far_last, factors, master, mine, mate, *refs):
    sources = refs[0:6]
    new_weights, steps, copies = refs[6:9]
    factors_v, master_v, weights_v, steps_v, joined, whole, blocks, made = refs[9:17]
    small_sems, whole_sems, block_sems, out_sems = refs[17:21]
    z, x, core = lax.axis_index(Z), lax.axis_index(X), lax.axis_index(C)
    small = [
        pltpu.make_async_copy(source, target, small_sems.at[i])
        for i, (source, target) in enumerate(
            ((factors, factors_v), (master, master_v))
        )
    ]
    owners, kept = [], []
    for far in range(4):
        for near in range(4):
            owner = jnp.where(
                core == 0,
                behind(z, far) * 4 + behind(x, near),
                behind(z, near) * 4 + behind(x, far),
            )
            row = pl.multiple_of(owner * 128, 128)
            if far == 2:
                kept.append(((far_first, far_last)[near // 2], near % 2, row))
            else:
                owners.append((sources[(0, 2, 0, 4)[far] + near // 2], near % 2, row))
    here = pl.multiple_of(core * 64, 64)
    there = pl.multiple_of((1 - core) * 64, 64)
    for j in range(3):
        for f in range(16):
            pltpu.make_async_copy(
                mine.at[f, j], whole.at[j, pl.ds(f * 128 + here, 64), :], whole_sems.at[j]
            ).start()
            pltpu.make_async_copy(
                mate.at[f, j], whole.at[j, pl.ds(f * 128 + there, 64), :], whole_sems.at[j]
            ).start()
        for source, slot, row in owners:
            pltpu.make_async_copy(source.at[slot, j], blocks.at[j, pl.ds(row, 128), :], block_sems.at[j]).start()
        if j == 0:
            for load in small:
                load.start()
    for source, slot, row in kept:
        for j in range(3):
            blocks[j, pl.ds(row, 128), :] = source[slot, j]
    sums = jnp.sum(squares[...], axis=(0, 1))
    inverse = lax.rsqrt(sums.reshape(1, 128)[0:1, 0:1] / entries + 1e-06)
    scale = 0.05 * inverse
    for j in range(3):
        for f in range(16):
            joined[j, 16 * f : 16 * f + 16, :] = gathered[f, j]
    small[0].wait()
    small[1].wait()
    stores = []
    for j in range(3):
        step = jnp.dot(factors_v[j], joined[j], preferred_element_type=F32) * inverse
        steps_v[j] = step
        weights_v[j] = master_v[j] - 0.05 * step
    stores.append(pltpu.make_async_copy(steps_v, steps, out_sems.at[6]))
    stores.append(pltpu.make_async_copy(weights_v, new_weights, out_sems.at[7]))
    for store in stores:
        store.start()
    for j in range(3):
        pltpu.make_async_copy(copies.at[j], whole.at[j], whole_sems.at[j]).wait()
        pltpu.make_async_copy(copies.at[j, 0:1536], blocks.at[j, 0:1536], block_sems.at[j]).wait()
        for half in range(2):
            for part in range(2):
                rows = pl.ds(1024 * half + 512 * part, 512)
                found = jnp.dot(whole[j, rows, :], joined[j], preferred_element_type=F32)
                made[j, rows, :] = (blocks[j, rows, :].astype(F32) - scale * found).astype(BF)
            rows = pl.ds(1024 * half, 1024)
            store = pltpu.make_async_copy(made.at[j, rows, :], copies.at[j, rows, :], out_sems.at[2 * j + half])
            store.start()
            stores.append(store)
    for store in stores:
        store.wait()


def on_device(
    normed_input,
    output_cotangent,
    query_grad,
    key_grad,
    attn_values,
    master_weights,
    factors,
    moments,
):
    (spread,) = call(
        spread_kernel,
        [jax.ShapeDtypeStruct((16, 3, 64, 256), BF)],
        [factors],
        [pltpu.VMEM((3, 64, 256), BF), pltpu.SemaphoreType.DMA, pltpu.SemaphoreType.DMA((16,))],
        mib=58,
        ins=hbm(1),
        out_specs=hbm(1),
    )
    mine = exchange(spread, FS)

    own = master_weights.astype(BF)
    top, bottom = own[:, :64], own[:, 64:]
    back_top = turn(top, True, 1)
    back_bottom = turn(bottom, True, 1)
    front_top = turn(top, True, -1)
    front_bottom = turn(bottom, True, -1)

    grads = gradients(normed_input, output_cotangent, query_grad, key_grad, attn_values)
    mine = after(mine, grads)
    mate = swap(mine)
    low = turn(after(back_top, mine), True, 1)
    high = turn(after(front_bottom, mine), True, -1)
    (parts,) = call(
        project_kernel,
        [jax.ShapeDtypeStruct((16, 3, 16, 256), BF)],
        [mine, mate, grads],
        [pltpu.VMEM((3, 2048, 256), BF)],
    )
    received = exchange(parts, FS)
    pair = jax.ShapeDtypeStruct((2, 3, 128, 256), BF)
    first, last, held = call(
        stack_kernel,
        [pair, pair, jax.ShapeDtypeStruct((3, 16, 256), F32)],
        [after(own, parts), back_top, back_bottom, low, high, front_top, front_bottom, moments],
    )
    back_first = turn(first, False, 1)
    back_last = turn(last, False, 1)
    front_first = turn(first, False, -1)
    front_last = turn(last, False, -1)
    normal, new_moments = call(
        moment_kernel,
        [jax.ShapeDtypeStruct((16, 3, 16, 256), BF), jax.ShapeDtypeStruct((3, 16, 256), F32)],
        [received, held],
    )
    gathered = exchange(normal, FS)
    far_first = turn(after(back_first, normal), False, 1)
    far_last = turn(after(front_last, normal), False, -1)
    (squares,) = call(join_kernel, [jax.ShapeDtypeStruct((8, 1, 128), F32)], [gathered])
    all_squares = exchange(squares, TP)
    entries = 3 * 256 * 2048
    shard = jax.ShapeDtypeStruct((3, 128, 256), F32)
    fixed = [factors, master_weights, mine, mate, first, last, back_first, back_last, front_first, front_last]
    args = [all_squares, gathered, far_first, far_last] + held_in_hbm(fixed)
    new_weights, steps, weight_copies = call(
        lambda *refs: update_kernel(entries, *refs),
        [shard, shard, jax.ShapeDtypeStruct((3, 2048, 256), BF)],
        args,
        [
            pltpu.VMEM((3, 128, 256), BF),
            pltpu.VMEM((3, 128, 256), F32),
            pltpu.VMEM((3, 128, 256), F32),
            pltpu.VMEM((3, 128, 256), F32),
            pltpu.VMEM((3, 256, 256), BF),
            pltpu.VMEM((3, 2048, 256), BF),
            pltpu.VMEM((3, 2048, 256), BF),
            pltpu.VMEM((3, 2048, 256), BF),
            pltpu.SemaphoreType.DMA((2,)),
            pltpu.SemaphoreType.DMA((3,)),
            pltpu.SemaphoreType.DMA((3,)),
            pltpu.SemaphoreType.DMA((8,)),
        ],
        mib=20,
        ins=vmem(4) + hbm(10),
        out_specs=hbm(3),
    )
    return (new_weights, weight_copies, steps, new_moments)


def solution(mesh):
    split = Mesh(mesh.devices.reshape(4, 4, 4, 2), (Z, X, Y, C))
    placed = (
        P(FS, None),
        P(FS, None),
        P(FS, TP),
        P(FS, TP),
        P(FS, TP),
        P(None, FS, TP),
        P(None, FS, None),
        P(None, FS, TP),
    )

    return jax.shard_map(
        on_device,
        mesh=split,
        in_specs=placed,
        out_specs=(P(None, FS, TP), P(None, None, TP), P(None, FS, TP), P(None, FS, TP)),
        check_vma=False,
    )
```

time: 106 us -> 100 us (0.943)
  Pallas kernels: 33.6 us -> 22.4 us
  starting transfers between devices: 25.9 us -> 34.2 us
  blocking collectives: 14.4 us -> 12 us
  waiting for transfers between devices: 24 us -> 25.8 us
  other arithmetic: 1.08 us -> 0.02 us
    all_to_all x3, waiting for transfers between devices: 9.08 us -> 25.1 us  [exchange(): return lax.all_to_all(value, axes, 0, 0, tiled=True)]
    ppermute x8 -> x12, waiting for transfers between devices: 15 us -> 0.67 us  [turn(): return lax.ppermute(value, FS + TP, pairs)]
    pallas_call x7, Pallas kernels: 33.6 us -> 22.4 us  [call(): pl.pallas_call(kernel, out_shape=outs, in_specs=ins or vmem(len(args)), o...]
    ppermute x8 -> x12, starting transfers between devices: 8.7 us -> 18.2 us  [turn(): return lax.ppermute(value, FS + TP, pairs)]
    all_to_all x1, blocking collectives: 14.4 us -> 12 us  [exchange(): return lax.all_to_all(value, axes, 0, 0, tiled=True)]
    slice x4 -> x1, local copies, waits for them, and re-layouts: 2.06 us -> 0.02 us  [on_device(): top, bottom = (own[:, :64], own[:, 64:])]
    all_to_all x3, starting transfers between devices: 17.2 us -> 16 us  [exchange(): return lax.all_to_all(value, axes, 0, 0, tiled=True)]
    unnamed x20 -> x24, local copies, waits for them, and re-layouts: 2.53 us -> 3.59 us
  transfers between devices with their start and end apart: 12 -> 16, of which waited for: 8 -> 4; matrix products, arithmetic and copies ran while one was open for 3% -> 0% of each run, Pallas kernels for 24% -> 15%
where the time goes in v2:
time: 100 us; the launch traced here: 98.9 us
  starting transfers between devices  34.2 us (34%)
  waiting for transfers between devices  25.8 us (26%)
  Pallas kernels  22.4 us (22%)
  blocking collectives  12 us (12%)
  local copies, waits for them, and re-layouts  3.61 us (4%)
    all_to_all x3, waiting for transfers between devices, exchange(): return lax.all_to_all(value, axes, 0, 0, tiled=True)  25.1 us
    pallas_call x7, Pallas kernels, call(): pl.pallas_call(kernel, out_shape=outs, in_specs=ins or vmem(len(args)), o...  22.4 us
    ppermute x12, starting transfers between devices, turn(): return lax.ppermute(value, FS + TP, pairs)  18.2 us
    all_to_all x3, starting transfers between devices, exchange(): return lax.all_to_all(value, axes, 0, 0, tiled=True)  16 us
    all_to_all x1, blocking collectives, exchange(): return lax.all_to_all(value, axes, 0, 0, tiled=True)  12 us
    unnamed x24, local copies, waits for them, and re-layouts  3.59 us
  transfers between devices with their start and end apart: 16, of which 4 were waited for; matrix products, arithmetic and copies ran while one was open for 0% of the time, Pallas kernels for 15%

profile of v2, /device:TPU:0, one launch (start us, length us, event | category | flops | bytes accessed | tf_op | source)
XLA Modules:
  0.0 98.9 jit_solution(6357250765931493677)
XLA Ops:
  0.6 2.2 %shard_map.111 = bf16[16,3,64,256]{3,2,1,0:T(8,128)(2,1)} custom-call(bf16[3,128,256]{2,1,0:T(8,128)(2,1)} %refs_4_.1), custom_call_target="tpu_custom_call" | custom-call | tf_op jit(solution)/shard_map/pallas_call | solution.py:46
  2.9 8.0 %all-to-all-start = ((bf16[16,3,64,256]{3,2,1,0:T(8,128)(2,1)}), bf16[16,3,64,256]{3,2,1,0:T(8,128)(2,1)S(1)}, u32[]{:S(2)}, u32[]{:S(2)}) async-start(bf16[16,3,64,256]{3,2,1,0:T(8,128)(2,1)} %shard_map.111), calls=%async_computation | async-start | bytes 3145728 | tf_op jit(solution)/shard_map/all_to_all | solution.py:34
  10.9 0.0 copy-start.7
  10.9 11.3 %shard_map.112.grads = bf16[3,256,2048]{2,1,0:T(8,128)(2,1)S(1)} custom-call(bf16[2048,2048]{1,0:T(8,128)(2,1)} %first.1, bf16[2048,2048]{1,0:T(8,128)(2,1)} %second.1, bf16[2048,256]{1,0:T(8,128)(2,1)} %q.1, bf16[2048,256]{1,0:T(8,128)(2,1)} %k.1, bf16[2048,256]{1,0:T(8,128)(2,1)} %v.1), custom_call_target="tpu_custom_call" | custom-call | tf_op jit(solution)/shard_map/pallas_call | solution.py:46
  22.2 0.0 copy-start.1
  22.2 1.7 %copy-done.1 = bf16[3,256,2048]{2,1,0:T(8,128)(2,1)} copy-done((bf16[3,256,2048]{2,1,0:T(8,128)(2,1)}, bf16[3,256,2048]{2,1,0:T(8,128)(2,1)S(1)}, u32[]{:S(2)}) %copy-start.1) | copy-done | bytes 3145752
  23.8 11.6 %all-to-all-done.mine.refs_6_ = bf16[16,3,64,256]{3,2,1,0:T(8,128)(2,1)S(1)} async-done(((bf16[16,3,64,256]{3,2,1,0:T(8,128)(2,1)}), bf16[16,3,64,256]{3,2,1,0:T(8,128)(2,1)S(1)}, u32[]{:S(2)}, u32[]{:S(2)}) %all-to-all-start) | async-done | bytes 1572896 | tf_op jit(solution)/shard_map/all_to_all | solution.py:34
  35.4 0.0 collective-permute-start
  35.4 0.0 copy-start.6
  35.5 0.1 collective-permute-start.4
  35.6 2.0 %collective-permute-start.1 = (bf16[3,64,256]{2,1,0:T(8,128)(2,1)S(1)}, bf16[3,64,256]{2,1,0:T(8,128)(2,1)S(1)}, u32[]{:S(2)}, u32[]{:S(2)}) collective-permute-start(bf16[3,64,256]{2,1,0:T(8,128)(2,1)S(1)} %get-tuple-element.33), channel_id=1, source_target_pairs={{0,8},{1,33},{2,10},{3,35},{4,12},{5,37},{6,14},{7,39},{8,16},{9,4... | collective-permute-start | bytes 294920 | tf_op jit(solution)/shard_map/ppermute | solution.py:30
  37.6 0.0 collective-permute-start.2
  37.6 3.2 %collective-permute-start.6 = (bf16[3,64,256]{2,1,0:T(8,128)(2,1)S(1)}, bf16[3,64,256]{2,1,0:T(8,128)(2,1)S(1)}, u32[]{:S(2)}, u32[]{:S(2)}) collective-permute-start(bf16[3,64,256]{2,1,0:T(8,128)(2,1)S(1)} %get-tuple-element.33), channel_id=1, source_target_pairs={{0,24},{1,97},{2,26},{3,99},{4,28},{5,101},{6,30},{7,103},{8,0},{9... | collective-permute-start | bytes 294920 | tf_op jit(solution)/shard_map/ppermute | solution.py:30
  40.8 0.0 collective-permute-done.4.front_bottom
  40.8 0.6 collective-permute-done.1.back_top
  41.5 0.7 collective-permute-start.3
  42.2 2.5 %collective-permute-start.5 = (bf16[3,64,256]{2,1,0:T(8,128)(2,1)S(1)}, bf16[3,64,256]{2,1,0:T(8,128)(2,1)S(1)}, u32[]{:S(2)}, u32[]{:S(2)}) collective-permute-start(bf16[3,64,256]{2,1,0:T(8,128)(2,1)S(1)} %collective-permute-done.4.front_bottom), channel_id=1, source_target_pairs={{0,24},{1,97},{2,26},{3,99},{4,28},{5,101},{6,30},{7,103},{8,0},{9... | collective-permute-start | bytes 294920 | tf_op jit(solution)/shard_map/ppermute | solution.py:30
  44.7 0.0 collective-permute-done.mate.refs_7_
  44.7 1.9 %copy-done.2 = bf16[3,256,2048]{2,1,0:T(8,128)(2,1)S(1)} copy-done((bf16[3,256,2048]{2,1,0:T(8,128)(2,1)S(1)}, bf16[3,256,2048]{2,1,0:T(8,128)(2,1)}, u32[]{:S(2)}) %copy-start.2) | copy-done | bytes 3145752
  46.6 2.0 %shard_map.113 = bf16[16,3,16,256]{3,2,1,0:T(8,128)(2,1)} custom-call(bf16[16,3,64,256]{3,2,1,0:T(8,128)(2,1)S(1)} %all-to-all-done.mine.refs_6_, bf16[16,3,64,256]{3,2,1,0:T(8,128)(2,1)S(1)} %collective-permute-done.mate.refs_7_, bf16[3,256,2048]{2,1,0:T(8,128)(2,1)S(1)} %copy-done.2), custom_call_target="tpu_custom_call" | custom-call | tf_op jit(solution)/shard_map/pallas_call | solution.py:46
  48.6 0.0 collective-permute-done.2.back_bottom
  48.6 0.0 collective-permute-done.6.front_top
  48.6 0.0 collective-permute-done.3.low
  48.7 0.0 collective-permute-done.5.high
  48.7 0.1 shard_map.114
  48.7 0.0 copy-start.4
  48.8 0.0 copy-start.5
  48.8 0.4 collective-permute-start.7
  49.2 2.9 %collective-permute-start.9 = (bf16[2,3,128,256]{3,2,1,0:T(8,128)(2,1)S(1)}, bf16[2,3,128,256]{3,2,1,0:T(8,128)(2,1)S(1)}, u32[]{:S(2)}, u32[]{:S(2)}) collective-permute-start(bf16[2,3,128,256]{3,2,1,0:T(8,128)(2,1)S(1)} %get-tuple-element.26.refs_9_), channel_id=1, source_target_pairs={{0,96},{1,25},{2,98},{3,27},{4,100},{5,29},{6,102},{7,31},{8,104},... | collective-permute-start | bytes 1179656 | tf_op jit(solution)/shard_map/ppermute | solution.py:30
  52.1 3.6 %all-to-all-start.1 = ((bf16[16,3,16,256]{3,2,1,0:T(8,128)(2,1)}), bf16[16,3,16,256]{3,2,1,0:T(8,128)(2,1)S(1)}, u32[]{:S(2)}, u32[]{:S(2)}) async-start(bf16[16,3,16,256]{3,2,1,0:T(8,128)(2,1)} %shard_map.113), calls=%async_computation.1 | async-start | bytes 786432 | tf_op jit(solution)/shard_map/all_to_all | solution.py:34
  55.6 3.1 %collective-permute-start.12 = (bf16[2,3,128,256]{3,2,1,0:T(8,128)(2,1)S(1)}, bf16[2,3,128,256]{3,2,1,0:T(8,128)(2,1)S(1)}, u32[]{:S(2)}, u32[]{:S(2)}) collective-permute-start(bf16[2,3,128,256]{3,2,1,0:T(8,128)(2,1)S(1)} %get-tuple-element.24.refs_8_), channel_id=1, source_target_pairs={{0,96},{1,25},{2,98},{3,27},{4,100},{5,29},{6,102},{7,31},{8,104},... | collective-permute-start | bytes 1179656 | tf_op jit(solution)/shard_map/ppermute | solution.py:30
  58.7 0.0 collective-permute-start.11
  58.7 8.4 %all-to-all-done.1.parts = bf16[16,3,16,256]{3,2,1,0:T(8,128)(2,1)S(1)} async-done(((bf16[16,3,16,256]{3,2,1,0:T(8,128)(2,1)}), bf16[16,3,16,256]{3,2,1,0:T(8,128)(2,1)S(1)}, u32[]{:S(2)}, u32[]{:S(2)}) %all-to-all-start.1) | async-done | bytes 393248 | tf_op jit(solution)/shard_map/all_to_all | solution.py:34
  67.1 0.7 shard_map.115
  67.8 0.0 collective-permute-done.7.refs_10_
  67.8 0.0 collective-permute-start.8
  67.8 0.0 collective-permute-done.9.refs_13_
  67.8 3.2 %collective-permute-start.10 = (bf16[2,3,128,256]{3,2,1,0:T(8,128)(2,1)S(1)}, bf16[2,3,128,256]{3,2,1,0:T(8,128)(2,1)S(1)}, u32[]{:S(2)}, u32[]{:S(2)}) collective-permute-start(bf16[2,3,128,256]{3,2,1,0:T(8,128)(2,1)S(1)} %collective-permute-done.9.refs_13_), channel_id=1, source_target_pairs={{0,96},{1,25},{2,98},{3,27},{4,100},{5,29},{6,102},{7,31},{8,104},... | collective-permute-start | bytes 1179656 | tf_op jit(solution)/shard_map/ppermute | solution.py:30
  71.0 12.0 %all_to_all.20.gathered.refs_1_ = bf16[16,3,16,256]{3,2,1,0:T(8,128)(2,1)S(1)} all-to-all(bf16[16,3,16,256]{3,2,1,0:T(8,128)(2,1)S(1)} %get-tuple-element.23), channel_id=1, replica_groups=mesh['fs_0'=4,'fs_1'=4,'tp_0'=4,'tp_1'=2] {'fs_0','fs_1'}, dimensions={0} | all-to-all | bytes 786432 | tf_op jit(solution)/shard_map/all_to_all | solution.py:34
  83.0 0.7 shard_map.116
  83.8 4.5 %all-to-all-start.3 = ((f32[8,1,128]{2,1,0:T(1,128)}), f32[8,1,128]{2,1,0:T(1,128)S(1)}, u32[]{:S(2)}, u32[]{:S(2)}) async-start(f32[8,1,128]{2,1,0:T(1,128)} %shard_map.116), calls=%async_computation.3 | async-start | bytes 8192 | tf_op jit(solution)/shard_map/all_to_all | solution.py:34
  88.2 0.0 collective-permute-done.12.refs_12_
  88.3 0.0 collective-permute-done.11.refs_11_
  88.3 0.0 copy-start.11
  88.3 5.2 %all-to-all-done.3.refs_0_ = f32[8,1,128]{2,1,0:T(1,128)S(1)} async-done(((f32[8,1,128]{2,1,0:T(1,128)}), f32[8,1,128]{2,1,0:T(1,128)S(1)}, u32[]{:S(2)}, u32[]{:S(2)}) %all-to-all-start.3) | async-done | bytes 4128 | tf_op jit(solution)/shard_map/all_to_all | solution.py:34
  93.5 0.0 collective-permute-done.8.refs_2_
  93.5 0.0 collective-permute-done.10.refs_3_
  93.5 5.4 %shard_map.117 = (f32[3,128,256]{2,1,0:T(8,128)}, f32[3,128,256]{2,1,0:T(8,128)}, bf16[3,2048,256]{2,1,0:T(8,128)(2,1)}) custom-call(f32[8,1,128]{2,1,0:T(1,128)S(1)} %all-to-all-done.3.refs_0_, bf16[16,3,16,256]{3,2,1,0:T(8,128)(2,1)S(1)} %all_to_all.20.gathered.refs_1_, bf16[2,3,128,256]{3,2,1,0:T(8,128)(2,1)S(1)} %collective-permute-done.8.refs_2_, ...), custom_call_target="tpu_custom_call" | custom-call | tf_op jit(solution)/shard_map/pallas_call | solution.py:46
  (18 shorter events, 0.1 us)
Async XLA Ops:
  2.9 32.5 %all-to-all-start = ((bf16[16,3,64,256]{3,2,1,0:T(8,128)(2,1)}), bf16[16,3,64,256]{3,2,1,0:T(8,128)(2,1)S(1)}, u32[]{:S(2)}, u32[]{:S(2)}) async-start(bf16[16,3,64,256]{3,2,1,0:T(8,128)(2,1)} %shard_map.111), calls=%async_computation | async-start | bytes 3145728 | tf_op jit(solution)/shard_map/all_to_all | solution.py:34
  10.9 24.5 %copy-start.7 = (f32[3,128,256]{2,1,0:T(8,128)S(1)}, f32[3,128,256]{2,1,0:T(8,128)}, u32[]{:S(2)}) copy-start(f32[3,128,256]{2,1,0:T(8,128)} %refs_5_.1) | copy-start | bytes 1179652
  22.2 1.7 %copy-start.1 = (bf16[3,256,2048]{2,1,0:T(8,128)(2,1)}, bf16[3,256,2048]{2,1,0:T(8,128)(2,1)S(1)}, u32[]{:S(2)}) copy-start(bf16[3,256,2048]{2,1,0:T(8,128)(2,1)S(1)} %shard_map.112.grads) | copy-start | bytes 9437188
  35.4 13.2 %copy-start = (bf16[16,3,64,256]{3,2,1,0:T(8,128)(2,1)}, bf16[16,3,64,256]{3,2,1,0:T(8,128)(2,1)S(1)}, u32[]{:S(2)}) copy-start(bf16[16,3,64,256]{3,2,1,0:T(8,128)(2,1)S(1)} %all-to-all-done.mine.refs_6_) | copy-start | bytes 4718596
  35.4 9.3 %collective-permute-start = (bf16[16,3,64,256]{3,2,1,0:T(8,128)(2,1)S(1)}, bf16[16,3,64,256]{3,2,1,0:T(8,128)(2,1)S(1)}, u32[]{:S(2)}, u32[]{:S(2)}) collective-permute-start(bf16[16,3,64,256]{3,2,1,0:T(8,128)(2,1)S(1)} %all-to-all-done.mine.refs_6_), channel_id=1, source_target_pairs={{0,1},{1,0},{2,3},{3,2},{4,5},{5,4},{6,7},{7,6},{8,9},{9,8},{10,11... | collective-permute-start | bytes 4718600 | tf_op jit(solution)/shard_map/ppermute | solution.py:18
  35.4 13.2 %copy-start.6 = (f32[3,16,256]{2,1,0:T(8,128)S(1)}, f32[3,16,256]{2,1,0:T(8,128)}, u32[]{:S(2)}) copy-start(f32[3,16,256]{2,1,0:T(8,128)} %moments.1) | copy-start | bytes 147460
  35.5 5.3 %collective-permute-start.4 = (bf16[3,64,256]{2,1,0:T(8,128)(2,1)S(1)}, bf16[3,64,256]{2,1,0:T(8,128)(2,1)S(1)}, u32[]{:S(2)}, u32[]{:S(2)}) collective-permute-start(bf16[3,64,256]{2,1,0:T(8,128)(2,1)S(1)} %get-tuple-element.32), channel_id=1, source_target_pairs={{0,24},{1,97},{2,26},{3,99},{4,28},{5,101},{6,30},{7,103},{8,0},{9... | collective-permute-start | bytes 294920 | tf_op jit(solution)/shard_map/ppermute | solution.py:30
  35.6 5.9 %collective-permute-start.1 = (bf16[3,64,256]{2,1,0:T(8,128)(2,1)S(1)}, bf16[3,64,256]{2,1,0:T(8,128)(2,1)S(1)}, u32[]{:S(2)}, u32[]{:S(2)}) collective-permute-start(bf16[3,64,256]{2,1,0:T(8,128)(2,1)S(1)} %get-tuple-element.33), channel_id=1, source_target_pairs={{0,8},{1,33},{2,10},{3,35},{4,12},{5,37},{6,14},{7,39},{8,16},{9,4... | collective-permute-start | bytes 294920 | tf_op jit(solution)/shard_map/ppermute | solution.py:30
  37.6 11.1 %collective-permute-start.2 = (bf16[3,64,256]{2,1,0:T(8,128)(2,1)S(1)}, bf16[3,64,256]{2,1,0:T(8,128)(2,1)S(1)}, u32[]{:S(2)}, u32[]{:S(2)}) collective-permute-start(bf16[3,64,256]{2,1,0:T(8,128)(2,1)S(1)} %get-tuple-element.32), channel_id=1, source_target_pairs={{0,8},{1,33},{2,10},{3,35},{4,12},{5,37},{6,14},{7,39},{8,16},{9,4... | collective-permute-start | bytes 294920 | tf_op jit(solution)/shard_map/ppermute | solution.py:30
  37.6 11.0 %collective-permute-start.6 = (bf16[3,64,256]{2,1,0:T(8,128)(2,1)S(1)}, bf16[3,64,256]{2,1,0:T(8,128)(2,1)S(1)}, u32[]{:S(2)}, u32[]{:S(2)}) collective-permute-start(bf16[3,64,256]{2,1,0:T(8,128)(2,1)S(1)} %get-tuple-element.33), channel_id=1, source_target_pairs={{0,24},{1,97},{2,26},{3,99},{4,28},{5,101},{6,30},{7,103},{8,0},{9... | collective-permute-start | bytes 294920 | tf_op jit(solution)/shard_map/ppermute | solution.py:30
  41.5 7.2 %collective-permute-start.3 = (bf16[3,64,256]{2,1,0:T(8,128)(2,1)S(1)}, bf16[3,64,256]{2,1,0:T(8,128)(2,1)S(1)}, u32[]{:S(2)}, u32[]{:S(2)}) collective-permute-start(bf16[3,64,256]{2,1,0:T(8,128)(2,1)S(1)} %collective-permute-done.1.back_top), channel_id=1, source_target_pairs={{0,8},{1,33},{2,10},{3,35},{4,12},{5,37},{6,14},{7,39},{8,16},{9,4... | collective-permute-start | bytes 294920 | tf_op jit(solution)/shard_map/ppermute | solution.py:30
  42.2 6.5 %collective-permute-start.5 = (bf16[3,64,256]{2,1,0:T(8,128)(2,1)S(1)}, bf16[3,64,256]{2,1,0:T(8,128)(2,1)S(1)}, u32[]{:S(2)}, u32[]{:S(2)}) collective-permute-start(bf16[3,64,256]{2,1,0:T(8,128)(2,1)S(1)} %collective-permute-done.4.front_bottom), channel_id=1, source_target_pairs={{0,24},{1,97},{2,26},{3,99},{4,28},{5,101},{6,30},{7,103},{8,0},{9... | collective-permute-start | bytes 294920 | tf_op jit(solution)/shard_map/ppermute | solution.py:30
  44.7 1.9 %copy-start.2 = (bf16[3,256,2048]{2,1,0:T(8,128)(2,1)S(1)}, bf16[3,256,2048]{2,1,0:T(8,128)(2,1)}, u32[]{:S(2)}) copy-start(bf16[3,256,2048]{2,1,0:T(8,128)(2,1)} %copy-done.1) | copy-start | bytes 9437188
  46.6 2.0 %copy-start.3 = (bf16[16,3,64,256]{3,2,1,0:T(8,128)(2,1)}, bf16[16,3,64,256]{3,2,1,0:T(8,128)(2,1)S(1)}, u32[]{:S(2)}) copy-start(bf16[16,3,64,256]{3,2,1,0:T(8,128)(2,1)S(1)} %collective-permute-done.mate.refs_7_) | copy-start | bytes 4718596
  48.7 44.7 %copy-start.4 = (bf16[2,3,128,256]{3,2,1,0:T(8,128)(2,1)}, bf16[2,3,128,256]{3,2,1,0:T(8,128)(2,1)S(1)}, u32[]{:S(2)}) copy-start(bf16[2,3,128,256]{3,2,1,0:T(8,128)(2,1)S(1)} %get-tuple-element.24.refs_8_) | copy-start | bytes 1179652
  48.8 44.7 %copy-start.5 = (bf16[2,3,128,256]{3,2,1,0:T(8,128)(2,1)}, bf16[2,3,128,256]{3,2,1,0:T(8,128)(2,1)S(1)}, u32[]{:S(2)}) copy-start(bf16[2,3,128,256]{3,2,1,0:T(8,128)(2,1)S(1)} %get-tuple-element.26.refs_9_) | copy-start | bytes 1179652
  48.8 19.0 %collective-permute-start.7 = (bf16[2,3,128,256]{3,2,1,0:T(8,128)(2,1)S(1)}, bf16[2,3,128,256]{3,2,1,0:T(8,128)(2,1)S(1)}, u32[]{:S(2)}, u32[]{:S(2)}) collective-permute-start(bf16[2,3,128,256]{3,2,1,0:T(8,128)(2,1)S(1)} %get-tuple-element.24.refs_8_), channel_id=1, source_target_pairs={{0,32},{1,9},{2,34},{3,11},{4,36},{5,13},{6,38},{7,15},{8,40},{9,1... | collective-permute-start | bytes 1179656 | tf_op jit(solution)/shard_map/ppermute | solution.py:30
  49.2 18.6 %collective-permute-start.9 = (bf16[2,3,128,256]{3,2,1,0:T(8,128)(2,1)S(1)}, bf16[2,3,128,256]{3,2,1,0:T(8,128)(2,1)S(1)}, u32[]{:S(2)}, u32[]{:S(2)}) collective-permute-start(bf16[2,3,128,256]{3,2,1,0:T(8,128)(2,1)S(1)} %get-tuple-element.26.refs_9_), channel_id=1, source_target_pairs={{0,96},{1,25},{2,98},{3,27},{4,100},{5,29},{6,102},{7,31},{8,104},... | collective-permute-start | bytes 1179656 | tf_op jit(solution)/shard_map/ppermute | solution.py:30
  52.1 15.0 %all-to-all-start.1 = ((bf16[16,3,16,256]{3,2,1,0:T(8,128)(2,1)}), bf16[16,3,16,256]{3,2,1,0:T(8,128)(2,1)S(1)}, u32[]{:S(2)}, u32[]{:S(2)}) async-start(bf16[16,3,16,256]{3,2,1,0:T(8,128)(2,1)} %shard_map.113), calls=%async_computation.1 | async-start | bytes 786432 | tf_op jit(solution)/shard_map/all_to_all | solution.py:34
  55.6 32.6 %collective-permute-start.12 = (bf16[2,3,128,256]{3,2,1,0:T(8,128)(2,1)S(1)}, bf16[2,3,128,256]{3,2,1,0:T(8,128)(2,1)S(1)}, u32[]{:S(2)}, u32[]{:S(2)}) collective-permute-start(bf16[2,3,128,256]{3,2,1,0:T(8,128)(2,1)S(1)} %get-tuple-element.24.refs_8_), channel_id=1, source_target_pairs={{0,96},{1,25},{2,98},{3,27},{4,100},{5,29},{6,102},{7,31},{8,104},... | collective-permute-start | bytes 1179656 | tf_op jit(solution)/shard_map/ppermute | solution.py:30
  58.7 29.5 %collective-permute-start.11 = (bf16[2,3,128,256]{3,2,1,0:T(8,128)(2,1)S(1)}, bf16[2,3,128,256]{3,2,1,0:T(8,128)(2,1)S(1)}, u32[]{:S(2)}, u32[]{:S(2)}) collective-permute-start(bf16[2,3,128,256]{3,2,1,0:T(8,128)(2,1)S(1)} %get-tuple-element.26.refs_9_), channel_id=1, source_target_pairs={{0,32},{1,9},{2,34},{3,11},{4,36},{5,13},{6,38},{7,15},{8,40},{9,1... | collective-permute-start | bytes 1179656 | tf_op jit(solution)/shard_map/ppermute | solution.py:30
  67.8 25.7 %copy-start.8 = (bf16[2,3,128,256]{3,2,1,0:T(8,128)(2,1)}, bf16[2,3,128,256]{3,2,1,0:T(8,128)(2,1)S(1)}, u32[]{:S(2)}) copy-start(bf16[2,3,128,256]{3,2,1,0:T(8,128)(2,1)S(1)} %collective-permute-done.7.refs_10_) | copy-start | bytes 1179652
  67.8 25.7 %collective-permute-start.8 = (bf16[2,3,128,256]{3,2,1,0:T(8,128)(2,1)S(1)}, bf16[2,3,128,256]{3,2,1,0:T(8,128)(2,1)S(1)}, u32[]{:S(2)}, u32[]{:S(2)}) collective-permute-start(bf16[2,3,128,256]{3,2,1,0:T(8,128)(2,1)S(1)} %collective-permute-done.7.refs_10_), channel_id=1, source_target_pairs={{0,32},{1,9},{2,34},{3,11},{4,36},{5,13},{6,38},{7,15},{8,40},{9,1... | collective-permute-start | bytes 1179656 | tf_op jit(solution)/shard_map/ppermute | solution.py:30
  67.8 25.7 %copy-start.9 = (bf16[2,3,128,256]{3,2,1,0:T(8,128)(2,1)}, bf16[2,3,128,256]{3,2,1,0:T(8,128)(2,1)S(1)}, u32[]{:S(2)}) copy-start(bf16[2,3,128,256]{3,2,1,0:T(8,128)(2,1)S(1)} %collective-permute-done.9.refs_13_) | copy-start | bytes 1179652
  67.8 25.6 %collective-permute-start.10 = (bf16[2,3,128,256]{3,2,1,0:T(8,128)(2,1)S(1)}, bf16[2,3,128,256]{3,2,1,0:T(8,128)(2,1)S(1)}, u32[]{:S(2)}, u32[]{:S(2)}) collective-permute-start(bf16[2,3,128,256]{3,2,1,0:T(8,128)(2,1)S(1)} %collective-permute-done.9.refs_13_), channel_id=1, source_target_pairs={{0,96},{1,25},{2,98},{3,27},{4,100},{5,29},{6,102},{7,31},{8,104},... | collective-permute-start | bytes 1179656 | tf_op jit(solution)/shard_map/ppermute | solution.py:30
  83.8 9.7 %all-to-all-start.3 = ((f32[8,1,128]{2,1,0:T(1,128)}), f32[8,1,128]{2,1,0:T(1,128)S(1)}, u32[]{:S(2)}, u32[]{:S(2)}) async-start(f32[8,1,128]{2,1,0:T(1,128)} %shard_map.116), calls=%async_computation.3 | async-start | bytes 8192 | tf_op jit(solution)/shard_map/all_to_all | solution.py:34
  88.2 5.3 %copy-start.10 = (bf16[2,3,128,256]{3,2,1,0:T(8,128)(2,1)}, bf16[2,3,128,256]{3,2,1,0:T(8,128)(2,1)S(1)}, u32[]{:S(2)}) copy-start(bf16[2,3,128,256]{3,2,1,0:T(8,128)(2,1)S(1)} %collective-permute-done.12.refs_12_) | copy-start | bytes 1179652
  88.3 5.2 %copy-start.11 = (bf16[2,3,128,256]{3,2,1,0:T(8,128)(2,1)}, bf16[2,3,128,256]{3,2,1,0:T(8,128)(2,1)S(1)}, u32[]{:S(2)}) copy-start(bf16[2,3,128,256]{3,2,1,0:T(8,128)(2,1)S(1)} %collective-permute-done.11.refs_11_) | copy-start | bytes 1179652

commit v3 on v2

v3 whole, which is shorter than its diff:
```python
import jax
import jax.numpy as jnp
from jax import lax
from jax.experimental import pallas as pl
from jax.experimental.pallas import tpu as pltpu
from jax.sharding import Mesh
from jax.sharding import PartitionSpec as P


Z, X, Y, C = "fs_0", "fs_1", "tp_0", "tp_1"
FS = (Z, X)
TP = (Y, C)
BF = jnp.bfloat16
F32 = jnp.float32


def swap(value):
    return lax.ppermute(value, C, [(0, 1), (1, 0)])


def turn(value, first, by):
    pairs = []
    for z in range(4):
        for x in range(4):
            for y in range(4):
                for c in range(2):
                    along_x = (c == 0) == first
                    to_z, to_x = (z, (x + by) % 4) if along_x else ((z + by) % 4, x)
                    pairs.append((((z * 4 + x) * 4 + y) * 2 + c, ((to_z * 4 + to_x) * 4 + y) * 2 + c))
    return lax.ppermute(value, FS + TP, pairs)


def exchange(value, axes):
    return lax.all_to_all(value, axes, 0, 0, tiled=True)


def vmem(count):
    return [pl.BlockSpec(memory_space=pltpu.VMEM) for _ in range(count)]


def hbm(count):
    return [pl.BlockSpec(memory_space=pltpu.HBM) for _ in range(count)]


def call(kernel, outs, args, scratch=(), mib=16, ins=None, out_specs=None):
    return pl.pallas_call(
        kernel,
        out_shape=outs,
        in_specs=ins or vmem(len(args)),
        out_specs=out_specs or vmem(len(outs)),
        scratch_shapes=list(scratch),
        compiler_params=pltpu.CompilerParams(vmem_limit_bytes=mib * 1024 * 1024),
    )(*args)


def behind(index, by):
    return lax.rem(index - by + 4, 4)


def after(value, *others):
    return lax.optimization_barrier((value, *others))[0]


def spread_kernel(factors, out, half, sem, sems):
    lanes = pl.ds(pl.multiple_of(lax.axis_index(C) * 128, 128), 128)
    load = pltpu.make_async_copy(factors.at[:, :, lanes], half, sem)
    load.start()
    load.wait()
    moves = [pltpu.make_async_copy(half, out.at[f], sems.at[f]) for f in range(16)]
    for move in moves:
        move.start()
    for move in moves:
        move.wait()


def gradient_kernel(first, second, q, k, v, out, a, b, sides, made, left_sems, side_sems, out_sems):
    def loads(source, target, sem, cols):
        for i in range(4):
            rows = pl.ds(512 * i, 512)
            pltpu.make_async_copy(source.at[rows, cols], target.at[rows, cols], sem).start()

    def wait(source, target, sem, cols):
        pltpu.make_async_copy(source.at[:, cols], target.at[:, cols], sem).wait()

    full = pl.ds(0, 256)
    halves = (pl.ds(0, 1024), pl.ds(1024, 1024))
    loads(q, sides.at[0], side_sems.at[0], full)
    loads(first, a, left_sems.at[0], halves[0])
    loads(k, sides.at[1], side_sems.at[1], full)
    loads(first, a, left_sems.at[1], halves[1])
    loads(v, sides.at[2], side_sems.at[2], full)
    loads(second, b, left_sems.at[2], halves[0])
    loads(second, b, left_sems.at[3], halves[1])
    stores = []
    done = set()
    for step, (j, half) in enumerate(((0, 0), (1, 0), (0, 1), (1, 1), (2, 0), (2, 1))):
        side, left, block = ((q, first, a), (k, first, a), (v, second, b))[j]
        if j not in done:
            done.add(j)
            wait(side, sides.at[j], side_sems.at[j], full)
        part = 2 * (j // 2) + half
        if j != 1:
            wait(left, block, left_sems.at[part], halves[half])
        made[j, :, halves[half]] = lax.dot_general(
            sides[j], block[:, halves[half]], (((0,), (0,)), ((), ())), preferred_element_type=F32
        ).astype(BF)
        store = pltpu.make_async_copy(made.at[j, :, halves[half]], out.at[j, :, halves[half]], out_sems.at[step])
        store.start()
        stores.append(store)
    for store in stores:
        store.wait()


def held_in_hbm(values):
    return [pltpu.with_memory_space_constraint(v, pltpu.HBM) for v in values]


def gradients(*args):
    (out,) = call(
        gradient_kernel,
        [jax.ShapeDtypeStruct((3, 256, 2048), BF)],
        args,
        [
            pltpu.VMEM((2048, 2048), BF),
            pltpu.VMEM((2048, 2048), BF),
            pltpu.VMEM((3, 2048, 256), BF),
            pltpu.VMEM((3, 256, 2048), BF),
            pltpu.SemaphoreType.DMA((4,)),
            pltpu.SemaphoreType.DMA((3,)),
            pltpu.SemaphoreType.DMA((6,)),
        ],
        mib=58,
        ins=hbm(5),
        out_specs=hbm(1),
    )
    return out


def side_kernel(mine, grads, kept, part, sems):
    loads = [pltpu.make_async_copy(grads.at[j], kept.at[j], sems.at[j]) for j in range(3)]
    for load in loads:
        load.start()
    for j in range(3):
        loads[j].wait()
        whole = mine[:, j].reshape(2048, 128)
        part[j] = jnp.dot(kept[j], whole, preferred_element_type=F32).T.astype(BF)


def project_kernel(mate, grads, part, parts):
    core = lax.axis_index(C)
    here, there = core * 8, 8 - core * 8
    for j in range(3):
        whole = mate[:, j].reshape(2048, 128)
        other = jnp.dot(grads[j], whole, preferred_element_type=F32).T.astype(BF)
        for i in range(8):
            parts[here + i, j] = part[j, 16 * i : 16 * i + 16, :]
            parts[there + i, j] = other[16 * i : 16 * i + 16, :]


def moment_kernel(parts, held, spread, new_moments):
    for j in range(3):
        s = parts[0, j].astype(F32)
        for f in range(1, 16):
            s = s + parts[f, j].astype(F32)
        m = held[j] + 0.2 * s
        new_moments[j] = m
        rounded = m.astype(BF)
        for f in range(16):
            spread[f, j] = rounded


def join_kernel(gathered, squares):
    acc = jnp.zeros((16, 256), F32)
    for j in range(3):
        for f in range(16):
            wide = gathered[f, j].astype(F32)
            acc = acc + wide * wide
    squares[...] = jnp.broadcast_to(jnp.sum(acc, axis=(0, 1), keepdims=True).reshape(1, 1, 1), squares.shape)


def stack_kernel(own, back_top, back_bottom, low, high, front_top, front_bottom, moments, line, held, raw, sem):
    load = pltpu.make_async_copy(moments, raw, sem)
    load.start()
    line[0] = own[...]
    line[1, :, 0:64, :] = back_top[...]
    line[1, :, 64:128, :] = back_bottom[...]
    line[2, :, 0:64, :] = low[...]
    line[2, :, 64:128, :] = high[...]
    line[3, :, 0:64, :] = front_top[...]
    line[3, :, 64:128, :] = front_bottom[...]
    load.wait()
    held[...] = 0.8 * raw[...]


def update_kernel(entries, squares, gathered, far_first, far_last, factors, master, mine, mate, *refs):
    line, back, front = refs[0:3]
    new_weights, steps, copies = refs[3:6]
    factors_v, master_v, weights_v, steps_v, joined, whole, blocks, made = refs[6:14]
    small_sems, whole_sems, block_sems, out_sems = refs[14:18]
    z, x, core = lax.axis_index(Z), lax.axis_index(X), lax.axis_index(C)
    small = [
        pltpu.make_async_copy(source, target, small_sems.at[i])
        for i, (source, target) in enumerate(
            ((factors, factors_v), (master, master_v))
        )
    ]
    owners, kept = [], []
    for far in range(4):
        for near in range(4):
            owner = jnp.where(
                core == 0,
                behind(z, far) * 4 + behind(x, near),
                behind(z, near) * 4 + behind(x, far),
            )
            row = pl.multiple_of(owner * 128, 128)
            if far == 2:
                kept.append(((far_first, far_last)[near // 2], near % 2, row))
            else:
                owners.append(((line, back, None, front)[far], near, row))
    here = pl.ds(pl.multiple_of(core * 128, 128), 128)
    there = pl.ds(pl.multiple_of(128 - core * 128, 128), 128)
    whole_loads = []
    for j in range(3):
        for side, (source, lanes) in enumerate(((mine, here), (mate, there))):
            whole_loads.append(
                pltpu.make_async_copy(source.at[:, j], whole.at[j, :, :, lanes], whole_sems.at[j, side])
            )
    block_loads = []
    for i, (source, slot, row) in enumerate(owners):
        block_loads.append(pltpu.make_async_copy(source.at[slot], blocks.at[:, pl.ds(row, 128), :], block_sems.at[i]))
    for load in small + whole_loads[:2] + block_loads + whole_loads[2:]:
        load.start()
    for source, slot, row in kept:
        for j in range(3):
            blocks[j, pl.ds(row, 128), :] = source[slot, j]
    sums = jnp.sum(squares[...], axis=(0, 1))
    inverse = lax.rsqrt(sums.reshape(1, 128)[0:1, 0:1] / entries + 1e-06)
    scale = 0.05 * inverse
    for j in range(3):
        for f in range(16):
            joined[j, 16 * f : 16 * f + 16, :] = gathered[f, j]
    small[0].wait()
    small[1].wait()
    stores = []
    for j in range(3):
        step = jnp.dot(factors_v[j], joined[j], preferred_element_type=F32) * inverse
        steps_v[j] = step
        weights_v[j] = master_v[j] - 0.05 * step
    stores.append(pltpu.make_async_copy(steps_v, steps, out_sems.at[12]))
    stores.append(pltpu.make_async_copy(weights_v, new_weights, out_sems.at[13]))
    for store in stores:
        store.start()
    for load in block_loads:
        load.wait()
    for j in range(3):
        for load in whole_loads[2 * j : 2 * j + 2]:
            load.wait()
        for part in range(4):
            rows = pl.ds(512 * part, 512)
            side = whole[j, 4 * part : 4 * part + 4].reshape(512, 256)
            found = jnp.dot(side, joined[j], preferred_element_type=F32)
            made[j, rows, :] = (blocks[j, rows, :].astype(F32) - scale * found).astype(BF)
            if part % 2 == 1 or j == 2:
                rows = pl.ds(512 * part, 512) if j == 2 else pl.ds(512 * part - 512, 1024)
                store = pltpu.make_async_copy(made.at[j, rows, :], copies.at[j, rows, :], out_sems.at[4 * j + part])
                store.start()
                stores.append(store)
    for store in stores:
        store.wait()


def on_device(
    normed_input,
    output_cotangent,
    query_grad,
    key_grad,
    attn_values,
    master_weights,
    factors,
    moments,
):
    (spread,) = call(
        spread_kernel,
        [jax.ShapeDtypeStruct((16, 3, 128, 128), BF)],
        [factors],
        [pltpu.VMEM((3, 128, 128), BF), pltpu.SemaphoreType.DMA, pltpu.SemaphoreType.DMA((16,))],
        mib=58,
        ins=hbm(1),
        out_specs=hbm(1),
    )
    mine = exchange(spread, FS)

    own = master_weights.astype(BF)
    top, bottom = own[:, :64], own[:, 64:]
    back_top = turn(top, True, 1)
    back_bottom = turn(bottom, True, 1)
    front_top = turn(top, True, -1)
    front_bottom = turn(bottom, True, -1)

    grads = gradients(normed_input, output_cotangent, query_grad, key_grad, attn_values)
    mine = after(mine, grads)
    mate = swap(mine)
    low = turn(after(back_top, mine), True, 1)
    high = turn(after(front_bottom, mine), True, -1)
    kept, part = call(
        side_kernel,
        [jax.ShapeDtypeStruct((3, 256, 2048), BF), jax.ShapeDtypeStruct((3, 128, 256), BF)],
        [mine] + held_in_hbm([grads]),
        [pltpu.SemaphoreType.DMA((3,))],
        ins=vmem(1) + hbm(1),
    )
    (parts,) = call(
        project_kernel,
        [jax.ShapeDtypeStruct((16, 3, 16, 256), BF)],
        [mate, kept, part],
    )
    received = exchange(parts, FS)
    line, held = call(
        stack_kernel,
        [jax.ShapeDtypeStruct((4, 3, 128, 256), BF), jax.ShapeDtypeStruct((3, 16, 256), F32)],
        [after(own, parts), back_top, back_bottom, low, high, front_top, front_bottom] + held_in_hbm([moments]),
        [pltpu.VMEM((3, 16, 256), F32), pltpu.SemaphoreType.DMA],
        ins=vmem(7) + hbm(1),
    )
    back = turn(line, False, 1)
    front = turn(line, False, -1)
    normal, new_moments = call(
        moment_kernel,
        [jax.ShapeDtypeStruct((16, 3, 16, 256), BF), jax.ShapeDtypeStruct((3, 16, 256), F32)],
        [received, held],
    )
    gathered = exchange(normal, FS)
    far_first = turn(after(back, normal)[:2], False, 1)
    far_last = turn(after(front, normal)[2:], False, -1)
    (squares,) = call(join_kernel, [jax.ShapeDtypeStruct((8, 1, 128), F32)], [gathered])
    all_squares = exchange(squares, TP)
    entries = 3 * 256 * 2048
    shard = jax.ShapeDtypeStruct((3, 128, 256), F32)
    fixed = [factors, master_weights, mine, mate, line, back, front]
    args = [all_squares, gathered, far_first, far_last] + held_in_hbm(fixed)
    new_weights, steps, weight_copies = call(
        lambda *refs: update_kernel(entries, *refs),
        [shard, shard, jax.ShapeDtypeStruct((3, 2048, 256), BF)],
        args,
        [
            pltpu.VMEM((3, 128, 256), BF),
            pltpu.VMEM((3, 128, 256), F32),
            pltpu.VMEM((3, 128, 256), F32),
            pltpu.VMEM((3, 128, 256), F32),
            pltpu.VMEM((3, 256, 256), BF),
            pltpu.VMEM((3, 16, 128, 256), BF),
            pltpu.VMEM((3, 2048, 256), BF),
            pltpu.VMEM((3, 2048, 256), BF),
            pltpu.SemaphoreType.DMA((2,)),
            pltpu.SemaphoreType.DMA((3, 2)),
            pltpu.SemaphoreType.DMA((12,)),
            pltpu.SemaphoreType.DMA((14,)),
        ],
        mib=20,
        ins=vmem(4) + hbm(7),
        out_specs=hbm(3),
    )
    return (new_weights, weight_copies, steps, new_moments)


def solution(mesh):
    split = Mesh(mesh.devices.reshape(4, 4, 4, 2), (Z, X, Y, C))
    placed = (
        P(FS, None),
        P(FS, None),
        P(FS, TP),
        P(FS, TP),
        P(FS, TP),
        P(None, FS, TP),
        P(None, FS, None),
        P(None, FS, TP),
    )

    return jax.shard_map(
        on_device,
        mesh=split,
        in_specs=placed,
        out_specs=(P(None, FS, TP), P(None, None, TP), P(None, FS, TP), P(None, FS, TP)),
        check_vma=False,
    )
```

time: 100 us -> 99.7 us (level)
  blocking collectives: 12 us -> 39.3 us
  starting transfers between devices: 34.2 us -> 20.8 us
  waiting for transfers between devices: 25.8 us -> 13.2 us
  local copies, waits for them, and re-layouts: 3.61 us -> 0.09 us
  Pallas kernels: 22.4 us -> 24.4 us
    all_to_all x1 -> x3, blocking collectives: 12 us -> 39.3 us  [exchange(): return lax.all_to_all(value, axes, 0, 0, tiled=True)]
    all_to_all x3 -> x1, waiting for transfers between devices: 25.1 us -> 12.5 us  [exchange(): return lax.all_to_all(value, axes, 0, 0, tiled=True)]
    all_to_all x3 -> x1, starting transfers between devices: 16 us -> 8 us  [exchange(): return lax.all_to_all(value, axes, 0, 0, tiled=True)]
    ppermute x12 -> x10, starting transfers between devices: 18.2 us -> 12.8 us  [turn(): return lax.ppermute(value, FS + TP, pairs)]
    unnamed x24 -> x12, local copies, waits for them, and re-layouts: 3.59 us -> 0.03 us
    pallas_call x7 -> x8, Pallas kernels: 22.4 us -> 24.4 us  [call(): pl.pallas_call(kernel, out_shape=outs, in_specs=ins or vmem(len(args)), o...]
  transfers between devices with their start and end apart: 16 -> 12, of which waited for: 4 -> 2; matrix products, arithmetic and copies ran while one was open for 0% -> 0% of each run, Pallas kernels for 15% -> 17%
where the time goes in v3:
time: 99.7 us; the launch traced here: 98.7 us
  blocking collectives  39.3 us (39%)
  Pallas kernels  24.4 us (24%)
  starting transfers between devices  20.8 us (21%)
  waiting for transfers between devices  13.2 us (13%)
    all_to_all x3, blocking collectives, exchange(): return lax.all_to_all(value, axes, 0, 0, tiled=True)  39.3 us
    pallas_call x8, Pallas kernels, call(): pl.pallas_call(kernel, out_shape=outs, in_specs=ins or vmem(len(args)), o...  24.4 us
    ppermute x10, starting transfers between devices, turn(): return lax.ppermute(value, FS + TP, pairs)  12.8 us
    all_to_all x1, waiting for transfers between devices, exchange(): return lax.all_to_all(value, axes, 0, 0, tiled=True)  12.5 us
    all_to_all x1, starting transfers between devices, exchange(): return lax.all_to_all(value, axes, 0, 0, tiled=True)  8 us
  transfers between devices with their start and end apart: 12, of which 2 were waited for; matrix products, arithmetic and copies ran while one was open for 0% of the time, Pallas kernels for 17%

profile of v3, /device:TPU:0, one launch (start us, length us, event | category | flops | bytes accessed | tf_op | source)
XLA Modules:
  0.0 98.7 jit_solution(8931830779306182012)
XLA Ops:
  0.6 2.2 %shard_map.111 = bf16[16,3,128,128]{3,2,1,0:T(8,128)(2,1)} custom-call(bf16[3,128,256]{2,1,0:T(8,128)(2,1)} %refs_4_.1), custom_call_target="tpu_custom_call" | custom-call | tf_op jit(solution)/shard_map/pallas_call | solution.py:46
  2.9 8.0 %all-to-all-start = ((bf16[16,3,128,128]{3,2,1,0:T(8,128)(2,1)}), bf16[16,3,128,128]{3,2,1,0:T(8,128)(2,1)S(1)}, u32[]{:S(2)}, u32[]{:S(2)}) async-start(bf16[16,3,128,128]{3,2,1,0:T(8,128)(2,1)} %shard_map.111), calls=%async_computation | async-start | bytes 3145728 | tf_op jit(solution)/shard_map/all_to_all | solution.py:34
  10.9 0.0 copy-start.5
  10.9 12.0 %shard_map.112.grads = bf16[3,256,2048]{2,1,0:T(8,128)(2,1)} custom-call(bf16[2048,2048]{1,0:T(8,128)(2,1)} %first.1, bf16[2048,2048]{1,0:T(8,128)(2,1)} %second.1, bf16[2048,256]{1,0:T(8,128)(2,1)} %q.1, bf16[2048,256]{1,0:T(8,128)(2,1)} %k.1, bf16[2048,256]{1,0:T(8,128)(2,1)} %v.1), custom_call_target="tpu_custom_call" | custom-call | tf_op jit(solution)/shard_map/pallas_call | solution.py:46
  22.9 12.5 %all-to-all-done.mine.refs_6_ = bf16[16,3,128,128]{3,2,1,0:T(8,128)(2,1)S(1)} async-done(((bf16[16,3,128,128]{3,2,1,0:T(8,128)(2,1)}), bf16[16,3,128,128]{3,2,1,0:T(8,128)(2,1)S(1)}, u32[]{:S(2)}, u32[]{:S(2)}) %all-to-all-start) | async-done | bytes 1572896 | tf_op jit(solution)/shard_map/all_to_all | solution.py:34
  35.4 0.0 copy-start
  35.4 0.0 collective-permute-start
  35.4 0.0 copy-done.5
  35.4 0.1 collective-permute-start.4
  35.5 2.0 %collective-permute-start.1 = (bf16[3,64,256]{2,1,0:T(8,128)(2,1)S(1)}, bf16[3,64,256]{2,1,0:T(8,128)(2,1)S(1)}, u32[]{:S(2)}, u32[]{:S(2)}) collective-permute-start(bf16[3,64,256]{2,1,0:T(8,128)(2,1)S(1)} %get-tuple-element.35), channel_id=1, source_target_pairs={{0,8},{1,33},{2,10},{3,35},{4,12},{5,37},{6,14},{7,39},{8,16},{9,4... | collective-permute-start | bytes 294920 | tf_op jit(solution)/shard_map/ppermute | solution.py:30
  37.5 0.0 collective-permute-start.2
  37.6 3.2 %collective-permute-start.6 = (bf16[3,64,256]{2,1,0:T(8,128)(2,1)S(1)}, bf16[3,64,256]{2,1,0:T(8,128)(2,1)S(1)}, u32[]{:S(2)}, u32[]{:S(2)}) collective-permute-start(bf16[3,64,256]{2,1,0:T(8,128)(2,1)S(1)} %get-tuple-element.35), channel_id=1, source_target_pairs={{0,24},{1,97},{2,26},{3,99},{4,28},{5,101},{6,30},{7,103},{8,0},{9... | collective-permute-start | bytes 294920 | tf_op jit(solution)/shard_map/ppermute | solution.py:30
  40.8 0.0 collective-permute-done.4.front_bottom
  40.8 0.6 collective-permute-done.1.back_top
  41.4 0.7 collective-permute-start.3
  42.2 2.5 %collective-permute-start.5 = (bf16[3,64,256]{2,1,0:T(8,128)(2,1)S(1)}, bf16[3,64,256]{2,1,0:T(8,128)(2,1)S(1)}, u32[]{:S(2)}, u32[]{:S(2)}) collective-permute-start(bf16[3,64,256]{2,1,0:T(8,128)(2,1)S(1)} %collective-permute-done.4.front_bottom), channel_id=1, source_target_pairs={{0,24},{1,97},{2,26},{3,99},{4,28},{5,101},{6,30},{7,103},{8,0},{9... | collective-permute-start | bytes 294920 | tf_op jit(solution)/shard_map/ppermute | solution.py:30
  44.7 2.7 %shard_map.113 = (bf16[3,256,2048]{2,1,0:T(8,128)(2,1)S(1)}, bf16[3,128,256]{2,1,0:T(8,128)(2,1)S(1)}) custom-call(bf16[16,3,128,128]{3,2,1,0:T(8,128)(2,1)S(1)} %all-to-all-done.mine.refs_6_, bf16[3,256,2048]{2,1,0:T(8,128)(2,1)} %shard_map.112.grads), custom_call_target="tpu_custom_call" | custom-call | tf_op jit(solution)/shard_map/pallas_call | solution.py:46
  47.4 0.0 collective-permute-done.mate.refs_7_
  47.4 0.0 copy-start.1
  47.4 1.0 %shard_map.114 = bf16[16,3,16,256]{3,2,1,0:T(8,128)(2,1)S(1)} custom-call(bf16[16,3,128,128]{3,2,1,0:T(8,128)(2,1)S(1)} %collective-permute-done.mate.refs_7_, bf16[3,256,2048]{2,1,0:T(8,128)(2,1)S(1)} %get-tuple-element.20.grads, bf16[3,128,256]{2,1,0:T(8,128)(2,1)S(1)} %get-tuple-element.21.part), custom_call_target="tpu_custom_call" | custom-call | tf_op jit(solution)/shard_map/pallas_call | solution.py:46
  48.5 0.0 copy-done
  48.5 0.0 collective-permute-done.2.back_bottom
  48.5 0.0 collective-permute-done.6.front_top
  48.5 0.0 collective-permute-done.3.low
  48.5 0.0 collective-permute-done.5.high
  48.5 0.8 shard_map.115
  49.3 0.0 copy-start.2
  49.4 1.2 %collective-permute-start.9 = (bf16[4,3,128,256]{3,2,1,0:T(8,128)(2,1)S(1)}, bf16[4,3,128,256]{3,2,1,0:T(8,128)(2,1)S(1)}, u32[]{:S(2)}, u32[]{:S(2)}) collective-permute-start(bf16[4,3,128,256]{3,2,1,0:T(8,128)(2,1)S(1)} %get-tuple-element.27.refs_8_), channel_id=1, source_target_pairs={{0,96},{1,25},{2,98},{3,27},{4,100},{5,29},{6,102},{7,31},{8,104},... | collective-permute-start | bytes 2359304 | tf_op jit(solution)/shard_map/ppermute | solution.py:30
  50.6 0.9 collective-permute-start.7
  51.5 16.5 %all_to_all.20.parts = bf16[16,3,16,256]{3,2,1,0:T(8,128)(2,1)S(1)} all-to-all(bf16[16,3,16,256]{3,2,1,0:T(8,128)(2,1)S(1)} %shard_map.114), channel_id=1, replica_groups=mesh['fs_0'=4,'fs_1'=4,'tp_0'=4,'tp_1'=2] {'fs_0','fs_1'}, dimensions={0} | all-to-all | bytes 786432 | tf_op jit(solution)/shard_map/all_to_all | solution.py:34
  68.0 0.0 copy-done.1
  68.0 0.7 shard_map.116
  68.7 0.0 collective-permute-done.9.refs_10_
  68.7 0.0 copy-start.3
  68.7 0.3 collective-permute-start.10
  69.0 0.0 collective-permute-done.7.refs_9_
  69.0 0.0 copy-start.4
  69.0 1.9 %collective-permute-start.8 = (bf16[2,3,128,256]{3,2,1,0:T(8,128)(2,1)S(1)}, bf16[2,3,128,256]{3,2,1,0:T(8,128)(2,1)S(1)}, u32[]{:S(2)}, u32[]{:S(2)}) collective-permute-start(bf16[2,3,128,256]{3,2,1,0:T(8,128)(2,1)S(1)} %slice.14), channel_id=1, source_target_pairs={{0,32},{1,9},{2,34},{3,11},{4,36},{5,13},{6,38},{7,15},{8,40},{9,1... | collective-permute-start | bytes 1179656 | tf_op jit(solution)/shard_map/ppermute | solution.py:30
  70.9 13.2 %all_to_all.21.gathered.refs_1_ = bf16[16,3,16,256]{3,2,1,0:T(8,128)(2,1)S(1)} all-to-all(bf16[16,3,16,256]{3,2,1,0:T(8,128)(2,1)S(1)} %get-tuple-element.26), channel_id=1, replica_groups=mesh['fs_0'=4,'fs_1'=4,'tp_0'=4,'tp_1'=2] {'fs_0','fs_1'}, dimensions={0} | all-to-all | bytes 786432 | tf_op jit(solution)/shard_map/all_to_all | solution.py:34
  84.1 0.1 shard_map.117
  84.3 9.6 %all_to_all.22.refs_0_ = f32[8,1,128]{2,1,0:T(1,128)S(1)} all-to-all(f32[8,1,128]{2,1,0:T(1,128)S(1)} %shard_map.117), channel_id=1, replica_groups=mesh['fs_0'=4,'fs_1'=4,'tp_0'=4,'tp_1'=2] {'tp_0','tp_1'}, dimensions={0} | all-to-all | bytes 8192 | tf_op jit(solution)/shard_map/all_to_all | solution.py:34
  93.9 0.0 collective-permute-done.10.refs_3_
  93.9 0.0 collective-permute-done.8.refs_2_
  93.9 0.0 copy-done.2
  93.9 0.0 copy-done.3
  93.9 0.0 copy-done.4
  93.9 4.8 %shard_map.118 = (f32[3,128,256]{2,1,0:T(8,128)}, f32[3,128,256]{2,1,0:T(8,128)}, bf16[3,2048,256]{2,1,0:T(8,128)(2,1)}) custom-call(f32[8,1,128]{2,1,0:T(1,128)S(1)} %all_to_all.22.refs_0_, bf16[16,3,16,256]{3,2,1,0:T(8,128)(2,1)S(1)} %all_to_all.21.gathered.refs_1_, bf16[2,3,128,256]{3,2,1,0:T(8,128)(2,1)S(1)} %collective-permute-done.8.refs_2_, ...), custom_call_target="tpu_custom_call" | custom-call | tf_op jit(solution)/shard_map/pallas_call | solution.py:46
  (4 shorter events, 0.1 us)
Async XLA Ops:
  2.9 32.5 %all-to-all-start = ((bf16[16,3,128,128]{3,2,1,0:T(8,128)(2,1)}), bf16[16,3,128,128]{3,2,1,0:T(8,128)(2,1)S(1)}, u32[]{:S(2)}, u32[]{:S(2)}) async-start(bf16[16,3,128,128]{3,2,1,0:T(8,128)(2,1)} %shard_map.111), calls=%async_computation | async-start | bytes 3145728 | tf_op jit(solution)/shard_map/all_to_all | solution.py:34
  10.9 24.5 %copy-start.5 = (f32[3,128,256]{2,1,0:T(8,128)S(1)}, f32[3,128,256]{2,1,0:T(8,128)}, u32[]{:S(2)}) copy-start(f32[3,128,256]{2,1,0:T(8,128)} %refs_5_.1) | copy-start | bytes 1179652
  35.4 13.1 %copy-start = (bf16[16,3,128,128]{3,2,1,0:T(8,128)(2,1)}, bf16[16,3,128,128]{3,2,1,0:T(8,128)(2,1)S(1)}, u32[]{:S(2)}) copy-start(bf16[16,3,128,128]{3,2,1,0:T(8,128)(2,1)S(1)} %all-to-all-done.mine.refs_6_) | copy-start | bytes 4718596
  35.4 12.0 %collective-permute-start = (bf16[16,3,128,128]{3,2,1,0:T(8,128)(2,1)S(1)}, bf16[16,3,128,128]{3,2,1,0:T(8,128)(2,1)S(1)}, u32[]{:S(2)}, u32[]{:S(2)}) collective-permute-start(bf16[16,3,128,128]{3,2,1,0:T(8,128)(2,1)S(1)} %all-to-all-done.mine.refs_6_), channel_id=1, source_target_pairs={{0,1},{1,0},{2,3},{3,2},{4,5},{5,4},{6,7},{7,6},{8,9},{9,8},{10,11... | collective-permute-start | bytes 4718600 | tf_op jit(solution)/shard_map/ppermute | solution.py:18
  35.4 5.3 %collective-permute-start.4 = (bf16[3,64,256]{2,1,0:T(8,128)(2,1)S(1)}, bf16[3,64,256]{2,1,0:T(8,128)(2,1)S(1)}, u32[]{:S(2)}, u32[]{:S(2)}) collective-permute-start(bf16[3,64,256]{2,1,0:T(8,128)(2,1)S(1)} %get-tuple-element.34), channel_id=1, source_target_pairs={{0,24},{1,97},{2,26},{3,99},{4,28},{5,101},{6,30},{7,103},{8,0},{9... | collective-permute-start | bytes 294920 | tf_op jit(solution)/shard_map/ppermute | solution.py:30
  35.5 5.9 %collective-permute-start.1 = (bf16[3,64,256]{2,1,0:T(8,128)(2,1)S(1)}, bf16[3,64,256]{2,1,0:T(8,128)(2,1)S(1)}, u32[]{:S(2)}, u32[]{:S(2)}) collective-permute-start(bf16[3,64,256]{2,1,0:T(8,128)(2,1)S(1)} %get-tuple-element.35), channel_id=1, source_target_pairs={{0,8},{1,33},{2,10},{3,35},{4,12},{5,37},{6,14},{7,39},{8,16},{9,4... | collective-permute-start | bytes 294920 | tf_op jit(solution)/shard_map/ppermute | solution.py:30
  37.5 10.9 %collective-permute-start.2 = (bf16[3,64,256]{2,1,0:T(8,128)(2,1)S(1)}, bf16[3,64,256]{2,1,0:T(8,128)(2,1)S(1)}, u32[]{:S(2)}, u32[]{:S(2)}) collective-permute-start(bf16[3,64,256]{2,1,0:T(8,128)(2,1)S(1)} %get-tuple-element.34), channel_id=1, source_target_pairs={{0,8},{1,33},{2,10},{3,35},{4,12},{5,37},{6,14},{7,39},{8,16},{9,4... | collective-permute-start | bytes 294920 | tf_op jit(solution)/shard_map/ppermute | solution.py:30
  37.6 10.9 %collective-permute-start.6 = (bf16[3,64,256]{2,1,0:T(8,128)(2,1)S(1)}, bf16[3,64,256]{2,1,0:T(8,128)(2,1)S(1)}, u32[]{:S(2)}, u32[]{:S(2)}) collective-permute-start(bf16[3,64,256]{2,1,0:T(8,128)(2,1)S(1)} %get-tuple-element.35), channel_id=1, source_target_pairs={{0,24},{1,97},{2,26},{3,99},{4,28},{5,101},{6,30},{7,103},{8,0},{9... | collective-permute-start | bytes 294920 | tf_op jit(solution)/shard_map/ppermute | solution.py:30
  41.4 7.1 %collective-permute-start.3 = (bf16[3,64,256]{2,1,0:T(8,128)(2,1)S(1)}, bf16[3,64,256]{2,1,0:T(8,128)(2,1)S(1)}, u32[]{:S(2)}, u32[]{:S(2)}) collective-permute-start(bf16[3,64,256]{2,1,0:T(8,128)(2,1)S(1)} %collective-permute-done.1.back_top), channel_id=1, source_target_pairs={{0,8},{1,33},{2,10},{3,35},{4,12},{5,37},{6,14},{7,39},{8,16},{9,4... | collective-permute-start | bytes 294920 | tf_op jit(solution)/shard_map/ppermute | solution.py:30
  42.2 6.4 %collective-permute-start.5 = (bf16[3,64,256]{2,1,0:T(8,128)(2,1)S(1)}, bf16[3,64,256]{2,1,0:T(8,128)(2,1)S(1)}, u32[]{:S(2)}, u32[]{:S(2)}) collective-permute-start(bf16[3,64,256]{2,1,0:T(8,128)(2,1)S(1)} %collective-permute-done.4.front_bottom), channel_id=1, source_target_pairs={{0,24},{1,97},{2,26},{3,99},{4,28},{5,101},{6,30},{7,103},{8,0},{9... | collective-permute-start | bytes 294920 | tf_op jit(solution)/shard_map/ppermute | solution.py:30
  47.4 20.6 %copy-start.1 = (bf16[16,3,128,128]{3,2,1,0:T(8,128)(2,1)}, bf16[16,3,128,128]{3,2,1,0:T(8,128)(2,1)S(1)}, u32[]{:S(2)}) copy-start(bf16[16,3,128,128]{3,2,1,0:T(8,128)(2,1)S(1)} %collective-permute-done.mate.refs_7_) | copy-start | bytes 4718596
  49.3 44.5 %copy-start.2 = (bf16[4,3,128,256]{3,2,1,0:T(8,128)(2,1)}, bf16[4,3,128,256]{3,2,1,0:T(8,128)(2,1)S(1)}, u32[]{:S(2)}) copy-start(bf16[4,3,128,256]{3,2,1,0:T(8,128)(2,1)S(1)} %get-tuple-element.27.refs_8_) | copy-start | bytes 2359300
  49.4 19.3 %collective-permute-start.9 = (bf16[4,3,128,256]{3,2,1,0:T(8,128)(2,1)S(1)}, bf16[4,3,128,256]{3,2,1,0:T(8,128)(2,1)S(1)}, u32[]{:S(2)}, u32[]{:S(2)}) collective-permute-start(bf16[4,3,128,256]{3,2,1,0:T(8,128)(2,1)S(1)} %get-tuple-element.27.refs_8_), channel_id=1, source_target_pairs={{0,96},{1,25},{2,98},{3,27},{4,100},{5,29},{6,102},{7,31},{8,104},... | collective-permute-start | bytes 2359304 | tf_op jit(solution)/shard_map/ppermute | solution.py:30
  50.6 18.4 %collective-permute-start.7 = (bf16[4,3,128,256]{3,2,1,0:T(8,128)(2,1)S(1)}, bf16[4,3,128,256]{3,2,1,0:T(8,128)(2,1)S(1)}, u32[]{:S(2)}, u32[]{:S(2)}) collective-permute-start(bf16[4,3,128,256]{3,2,1,0:T(8,128)(2,1)S(1)} %get-tuple-element.27.refs_8_), channel_id=1, source_target_pairs={{0,32},{1,9},{2,34},{3,11},{4,36},{5,13},{6,38},{7,15},{8,40},{9,1... | collective-permute-start | bytes 2359304 | tf_op jit(solution)/shard_map/ppermute | solution.py:30
  68.7 25.2 %copy-start.3 = (bf16[4,3,128,256]{3,2,1,0:T(8,128)(2,1)}, bf16[4,3,128,256]{3,2,1,0:T(8,128)(2,1)S(1)}, u32[]{:S(2)}) copy-start(bf16[4,3,128,256]{3,2,1,0:T(8,128)(2,1)S(1)} %collective-permute-done.9.refs_10_) | copy-start | bytes 2359300
  68.7 25.1 %collective-permute-start.10 = (bf16[2,3,128,256]{3,2,1,0:T(8,128)(2,1)S(1)}, bf16[2,3,128,256]{3,2,1,0:T(8,128)(2,1)S(1)}, u32[]{:S(2)}, u32[]{:S(2)}) collective-permute-start(bf16[2,3,128,256]{3,2,1,0:T(8,128)(2,1)S(1)} %slice.15), channel_id=1, source_target_pairs={{0,96},{1,25},{2,98},{3,27},{4,100},{5,29},{6,102},{7,31},{8,104},... | collective-permute-start | bytes 1179656 | tf_op jit(solution)/shard_map/ppermute | solution.py:30
  69.0 24.9 %copy-start.4 = (bf16[4,3,128,256]{3,2,1,0:T(8,128)(2,1)}, bf16[4,3,128,256]{3,2,1,0:T(8,128)(2,1)S(1)}, u32[]{:S(2)}) copy-start(bf16[4,3,128,256]{3,2,1,0:T(8,128)(2,1)S(1)} %collective-permute-done.7.refs_9_) | copy-start | bytes 2359300
  69.0 24.8 %collective-permute-start.8 = (bf16[2,3,128,256]{3,2,1,0:T(8,128)(2,1)S(1)}, bf16[2,3,128,256]{3,2,1,0:T(8,128)(2,1)S(1)}, u32[]{:S(2)}, u32[]{:S(2)}) collective-permute-start(bf16[2,3,128,256]{3,2,1,0:T(8,128)(2,1)S(1)} %slice.14), channel_id=1, source_target_pairs={{0,32},{1,9},{2,34},{3,11},{4,36},{5,13},{6,38},{7,15},{8,40},{9,1... | collective-permute-start | bytes 1179656 | tf_op jit(solution)/shard_map/ppermute | solution.py:30

commit v4 on v3

--- a/solution.py
+++ b/solution.py
@@ -178,16 +178,11 @@
     squares[...] = jnp.broadcast_to(jnp.sum(acc, axis=(0, 1), keepdims=True).reshape(1, 1, 1), squares.shape)
 
 
-def stack_kernel(own, back_top, back_bottom, low, high, front_top, front_bottom, moments, line, held, raw, sem):
+def stack_kernel(own, near_back, opposite, near_front, moments, line, held, raw, sem):
     load = pltpu.make_async_copy(moments, raw, sem)
     load.start()
-    line[0] = own[...]
-    line[1, :, 0:64, :] = back_top[...]
-    line[1, :, 64:128, :] = back_bottom[...]
-    line[2, :, 0:64, :] = low[...]
-    line[2, :, 64:128, :] = high[...]
-    line[3, :, 0:64, :] = front_top[...]
-    line[3, :, 64:128, :] = front_bottom[...]
+    for i, block in enumerate((own, near_back, opposite, near_front)):
+        line[i] = block[...]
     load.wait()
     held[...] = 0.8 * raw[...]
 
@@ -291,17 +286,13 @@
     mine = exchange(spread, FS)
 
     own = master_weights.astype(BF)
-    top, bottom = own[:, :64], own[:, 64:]
-    back_top = turn(top, True, 1)
-    back_bottom = turn(bottom, True, 1)
-    front_top = turn(top, True, -1)
-    front_bottom = turn(bottom, True, -1)
+    near_back = turn(own, True, 1)
+    near_front = turn(own, True, -1)
+    opposite = turn(own, True, 2)
 
     grads = gradients(normed_input, output_cotangent, query_grad, key_grad, attn_values)
     mine = after(mine, grads)
     mate = swap(mine)
-    low = turn(after(back_top, mine), True, 1)
-    high = turn(after(front_bottom, mine), True, -1)
     kept, part = call(
         side_kernel,
         [jax.ShapeDtypeStruct((3, 256, 2048), BF), jax.ShapeDtypeStruct((3, 128, 256), BF)],
@@ -318,9 +309,9 @@
     line, held = call(
         stack_kernel,
         [jax.ShapeDtypeStruct((4, 3, 128, 256), BF), jax.ShapeDtypeStruct((3, 16, 256), F32)],
-        [after(own, parts), back_top, back_bottom, low, high, front_top, front_bottom] + held_in_hbm([moments]),
+        [after(own, parts), near_back, opposite, near_front] + held_in_hbm([moments]),
         [pltpu.VMEM((3, 16, 256), F32), pltpu.SemaphoreType.DMA],
-        ins=vmem(7) + hbm(1),
+        ins=vmem(4) + hbm(1),
     )
     back = turn(line, False, 1)
     front = turn(line, False, -1)

time: 99.7 us -> 95.2 us (0.955)
  starting transfers between devices: 20.8 us -> 14.4 us
  waiting for transfers between devices: 13.2 us -> 16 us
    ppermute x10 -> x7, starting transfers between devices: 12.8 us -> 6.35 us  [turn(): return lax.ppermute(value, FS + TP, pairs)]
    ppermute x10 -> x7, waiting for transfers between devices: 0.67 us -> 3.53 us  [turn(): return lax.ppermute(value, FS + TP, pairs)]
  transfers between devices with their start and end apart: 12 -> 9, of which waited for: 2 -> 3; matrix products, arithmetic and copies ran while one was open for 0% -> 0% of each run, Pallas kernels for 17% -> 18%
where the time goes in v4:
time: 95.2 us; the launch traced here: 94.1 us
  blocking collectives  38.4 us (40%)
  Pallas kernels  24.4 us (26%)
  waiting for transfers between devices  16 us (17%)
  starting transfers between devices  14.4 us (15%)
    all_to_all x3, blocking collectives, exchange(): return lax.all_to_all(value, axes, 0, 0, tiled=True)  38.4 us
    pallas_call x8, Pallas kernels, call(): pl.pallas_call(kernel, out_shape=outs, in_specs=ins or vmem(len(args)), o...  24.4 us
    all_to_all x1, waiting for transfers between devices, exchange(): return lax.all_to_all(value, axes, 0, 0, tiled=True)  12.5 us
    all_to_all x1, starting transfers between devices, exchange(): return lax.all_to_all(value, axes, 0, 0, tiled=True)  8 us
    ppermute x7, starting transfers between devices, turn(): return lax.ppermute(value, FS + TP, pairs)  6.35 us
    ppermute x7, waiting for transfers between devices, turn(): return lax.ppermute(value, FS + TP, pairs)  3.53 us
  transfers between devices with their start and end apart: 9, of which 3 were waited for; matrix products, arithmetic and copies ran while one was open for 0% of the time, Pallas kernels for 18%

profile of v4, /device:TPU:0, one launch (start us, length us, event | category | flops | bytes accessed | tf_op | source)
XLA Modules:
  0.0 94.1 jit_solution(12360788522267755068)
XLA Ops:
  0.6 2.2 %shard_map.111 = bf16[16,3,128,128]{3,2,1,0:T(8,128)(2,1)} custom-call(bf16[3,128,256]{2,1,0:T(8,128)(2,1)} %refs_4_.1), custom_call_target="tpu_custom_call" | custom-call | tf_op jit(solution)/shard_map/pallas_call | solution.py:46
  2.9 8.0 %all-to-all-start = ((bf16[16,3,128,128]{3,2,1,0:T(8,128)(2,1)}), bf16[16,3,128,128]{3,2,1,0:T(8,128)(2,1)S(1)}, u32[]{:S(2)}, u32[]{:S(2)}) async-start(bf16[16,3,128,128]{3,2,1,0:T(8,128)(2,1)} %shard_map.111), calls=%async_computation | async-start | bytes 3145728 | tf_op jit(solution)/shard_map/all_to_all | solution.py:34
  10.9 0.0 copy-start.5
  10.9 12.0 %shard_map.112.grads = bf16[3,256,2048]{2,1,0:T(8,128)(2,1)} custom-call(bf16[2048,2048]{1,0:T(8,128)(2,1)} %first.1, bf16[2048,2048]{1,0:T(8,128)(2,1)} %second.1, bf16[2048,256]{1,0:T(8,128)(2,1)} %q.1, bf16[2048,256]{1,0:T(8,128)(2,1)} %k.1, bf16[2048,256]{1,0:T(8,128)(2,1)} %v.1), custom_call_target="tpu_custom_call" | custom-call | tf_op jit(solution)/shard_map/pallas_call | solution.py:46
  22.9 12.5 %all-to-all-done.mine.refs_6_ = bf16[16,3,128,128]{3,2,1,0:T(8,128)(2,1)S(1)} async-done(((bf16[16,3,128,128]{3,2,1,0:T(8,128)(2,1)}), bf16[16,3,128,128]{3,2,1,0:T(8,128)(2,1)S(1)}, u32[]{:S(2)}, u32[]{:S(2)}) %all-to-all-start) | async-done | bytes 1572896 | tf_op jit(solution)/shard_map/all_to_all | solution.py:34
  35.4 0.0 copy-start
  35.4 0.0 collective-permute-start
  35.4 0.0 copy-done.5
  35.4 0.1 collective-permute-start.3
  35.5 1.0 %collective-permute-start.2 = (bf16[3,128,256]{2,1,0:T(8,128)(2,1)S(1)}, bf16[3,128,256]{2,1,0:T(8,128)(2,1)S(1)}, u32[]{:S(2)}, u32[]{:S(2)}) collective-permute-start(bf16[3,128,256]{2,1,0:T(8,128)(2,1)S(1)} %convert_element_type.3.own), channel_id=1, source_target_pairs={{0,16},{1,65},{2,18},{3,67},{4,20},{5,69},{6,22},{7,71},{8,24},{9,... | collective-permute-start | bytes 589832 | tf_op jit(solution)/shard_map/ppermute | solution.py:30
  36.5 1.1 %collective-permute-start.1 = (bf16[3,128,256]{2,1,0:T(8,128)(2,1)S(1)}, bf16[3,128,256]{2,1,0:T(8,128)(2,1)S(1)}, u32[]{:S(2)}, u32[]{:S(2)}) collective-permute-start(bf16[3,128,256]{2,1,0:T(8,128)(2,1)S(1)} %convert_element_type.3.own), channel_id=1, source_target_pairs={{0,8},{1,33},{2,10},{3,35},{4,12},{5,37},{6,14},{7,39},{8,16},{9,4... | collective-permute-start | bytes 589832 | tf_op jit(solution)/shard_map/ppermute | solution.py:30
  37.5 2.7 %shard_map.113 = (bf16[3,256,2048]{2,1,0:T(8,128)(2,1)S(1)}, bf16[3,128,256]{2,1,0:T(8,128)(2,1)S(1)}) custom-call(bf16[16,3,128,128]{3,2,1,0:T(8,128)(2,1)S(1)} %all-to-all-done.mine.refs_6_, bf16[3,256,2048]{2,1,0:T(8,128)(2,1)} %shard_map.112.grads), custom_call_target="tpu_custom_call" | custom-call | tf_op jit(solution)/shard_map/pallas_call | solution.py:46
  40.3 0.0 collective-permute-done.mate.refs_7_
  40.3 0.0 copy-start.1
  40.3 1.0 %shard_map.114 = bf16[16,3,16,256]{3,2,1,0:T(8,128)(2,1)S(1)} custom-call(bf16[16,3,128,128]{3,2,1,0:T(8,128)(2,1)S(1)} %collective-permute-done.mate.refs_7_, bf16[3,256,2048]{2,1,0:T(8,128)(2,1)S(1)} %get-tuple-element.18.grads, bf16[3,128,256]{2,1,0:T(8,128)(2,1)S(1)} %get-tuple-element.19.part), custom_call_target="tpu_custom_call" | custom-call | tf_op jit(solution)/shard_map/pallas_call | solution.py:46
  41.3 0.0 copy-done
  41.4 0.0 collective-permute-done.3.near_front
  41.4 1.5 %collective-permute-done.2.opposite = bf16[3,128,256]{2,1,0:T(8,128)(2,1)S(1)} collective-permute-done((bf16[3,128,256]{2,1,0:T(8,128)(2,1)S(1)}, bf16[3,128,256]{2,1,0:T(8,128)(2,1)S(1)}, u32[]{:S(2)}, u32[]{:S(2)}) %collective-permute-start.2) | collective-permute-done | bytes 196640 | tf_op jit(solution)/shard_map/ppermute | solution.py:30
  42.9 2.0 %collective-permute-done.1.near_back = bf16[3,128,256]{2,1,0:T(8,128)(2,1)S(1)} collective-permute-done((bf16[3,128,256]{2,1,0:T(8,128)(2,1)S(1)}, bf16[3,128,256]{2,1,0:T(8,128)(2,1)S(1)}, u32[]{:S(2)}, u32[]{:S(2)}) %collective-permute-start.1) | collective-permute-done | bytes 196640 | tf_op jit(solution)/shard_map/ppermute | solution.py:30
  44.9 0.8 shard_map.115
  45.7 0.0 copy-start.2
  45.7 1.2 %collective-permute-start.6 = (bf16[4,3,128,256]{3,2,1,0:T(8,128)(2,1)S(1)}, bf16[4,3,128,256]{3,2,1,0:T(8,128)(2,1)S(1)}, u32[]{:S(2)}, u32[]{:S(2)}) collective-permute-start(bf16[4,3,128,256]{3,2,1,0:T(8,128)(2,1)S(1)} %get-tuple-element.23.refs_8_), channel_id=1, source_target_pairs={{0,96},{1,25},{2,98},{3,27},{4,100},{5,29},{6,102},{7,31},{8,104},... | collective-permute-start | bytes 2359304 | tf_op jit(solution)/shard_map/ppermute | solution.py:30
  46.9 0.9 collective-permute-start.4
  47.8 16.5 %all_to_all.20.parts = bf16[16,3,16,256]{3,2,1,0:T(8,128)(2,1)S(1)} all-to-all(bf16[16,3,16,256]{3,2,1,0:T(8,128)(2,1)S(1)} %shard_map.114), channel_id=1, replica_groups=mesh['fs_0'=4,'fs_1'=4,'tp_0'=4,'tp_1'=2] {'fs_0','fs_1'}, dimensions={0} | all-to-all | bytes 786432 | tf_op jit(solution)/shard_map/all_to_all | solution.py:34
  64.3 0.0 copy-done.1
  64.3 0.7 shard_map.116
  65.0 0.0 collective-permute-done.6.refs_10_
  65.0 0.0 copy-start.3
  65.1 0.1 collective-permute-start.7
  65.2 0.0 collective-permute-done.4.refs_9_
  65.2 0.0 copy-start.4
  65.2 2.0 %collective-permute-start.5 = (bf16[2,3,128,256]{3,2,1,0:T(8,128)(2,1)S(1)}, bf16[2,3,128,256]{3,2,1,0:T(8,128)(2,1)S(1)}, u32[]{:S(2)}, u32[]{:S(2)}) collective-permute-start(bf16[2,3,128,256]{3,2,1,0:T(8,128)(2,1)S(1)} %slice.6), channel_id=1, source_target_pairs={{0,32},{1,9},{2,34},{3,11},{4,36},{5,13},{6,38},{7,15},{8,40},{9,1... | collective-permute-start | bytes 1179656 | tf_op jit(solution)/shard_map/ppermute | solution.py:30
  67.3 12.3 %all_to_all.21.gathered.refs_1_ = bf16[16,3,16,256]{3,2,1,0:T(8,128)(2,1)S(1)} all-to-all(bf16[16,3,16,256]{3,2,1,0:T(8,128)(2,1)S(1)} %get-tuple-element.22), channel_id=1, replica_groups=mesh['fs_0'=4,'fs_1'=4,'tp_0'=4,'tp_1'=2] {'fs_0','fs_1'}, dimensions={0} | all-to-all | bytes 786432 | tf_op jit(solution)/shard_map/all_to_all | solution.py:34
  79.6 0.1 shard_map.117
  79.8 9.6 %all_to_all.22.refs_0_ = f32[8,1,128]{2,1,0:T(1,128)S(1)} all-to-all(f32[8,1,128]{2,1,0:T(1,128)S(1)} %shard_map.117), channel_id=1, replica_groups=mesh['fs_0'=4,'fs_1'=4,'tp_0'=4,'tp_1'=2] {'tp_0','tp_1'}, dimensions={0} | all-to-all | bytes 8192 | tf_op jit(solution)/shard_map/all_to_all | solution.py:34
  89.3 0.0 collective-permute-done.7.refs_3_
  89.3 0.0 collective-permute-done.5.refs_2_
  89.3 0.0 copy-done.2
  89.3 0.0 copy-done.3
  89.4 0.0 copy-done.4
  89.4 4.8 %shard_map.118 = (f32[3,128,256]{2,1,0:T(8,128)}, f32[3,128,256]{2,1,0:T(8,128)}, bf16[3,2048,256]{2,1,0:T(8,128)(2,1)}) custom-call(f32[8,1,128]{2,1,0:T(1,128)S(1)} %all_to_all.22.refs_0_, bf16[16,3,16,256]{3,2,1,0:T(8,128)(2,1)S(1)} %all_to_all.21.gathered.refs_1_, bf16[2,3,128,256]{3,2,1,0:T(8,128)(2,1)S(1)} %collective-permute-done.5.refs_2_, ...), custom_call_target="tpu_custom_call" | custom-call | tf_op jit(solution)/shard_map/pallas_call | solution.py:46
  (3 shorter events, 0.1 us)
Async XLA Ops:
  2.9 32.5 %all-to-all-start = ((bf16[16,3,128,128]{3,2,1,0:T(8,128)(2,1)}), bf16[16,3,128,128]{3,2,1,0:T(8,128)(2,1)S(1)}, u32[]{:S(2)}, u32[]{:S(2)}) async-start(bf16[16,3,128,128]{3,2,1,0:T(8,128)(2,1)} %shard_map.111), calls=%async_computation | async-start | bytes 3145728 | tf_op jit(solution)/shard_map/all_to_all | solution.py:34
  10.9 24.5 %copy-start.5 = (f32[3,128,256]{2,1,0:T(8,128)S(1)}, f32[3,128,256]{2,1,0:T(8,128)}, u32[]{:S(2)}) copy-start(f32[3,128,256]{2,1,0:T(8,128)} %refs_5_.1) | copy-start | bytes 1179652
  35.4 5.9 %copy-start = (bf16[16,3,128,128]{3,2,1,0:T(8,128)(2,1)}, bf16[16,3,128,128]{3,2,1,0:T(8,128)(2,1)S(1)}, u32[]{:S(2)}) copy-start(bf16[16,3,128,128]{3,2,1,0:T(8,128)(2,1)S(1)} %all-to-all-done.mine.refs_6_) | copy-start | bytes 4718596
  35.4 4.9 %collective-permute-start = (bf16[16,3,128,128]{3,2,1,0:T(8,128)(2,1)S(1)}, bf16[16,3,128,128]{3,2,1,0:T(8,128)(2,1)S(1)}, u32[]{:S(2)}, u32[]{:S(2)}) collective-permute-start(bf16[16,3,128,128]{3,2,1,0:T(8,128)(2,1)S(1)} %all-to-all-done.mine.refs_6_), channel_id=1, source_target_pairs={{0,1},{1,0},{2,3},{3,2},{4,5},{5,4},{6,7},{7,6},{8,9},{9,8},{10,11... | collective-permute-start | bytes 4718600 | tf_op jit(solution)/shard_map/ppermute | solution.py:18
  35.4 5.9 %collective-permute-start.3 = (bf16[3,128,256]{2,1,0:T(8,128)(2,1)S(1)}, bf16[3,128,256]{2,1,0:T(8,128)(2,1)S(1)}, u32[]{:S(2)}, u32[]{:S(2)}) collective-permute-start(bf16[3,128,256]{2,1,0:T(8,128)(2,1)S(1)} %convert_element_type.3.own), channel_id=1, source_target_pairs={{0,24},{1,97},{2,26},{3,99},{4,28},{5,101},{6,30},{7,103},{8,0},{9... | collective-permute-start | bytes 589832 | tf_op jit(solution)/shard_map/ppermute | solution.py:30
  35.5 7.4 %collective-permute-start.2 = (bf16[3,128,256]{2,1,0:T(8,128)(2,1)S(1)}, bf16[3,128,256]{2,1,0:T(8,128)(2,1)S(1)}, u32[]{:S(2)}, u32[]{:S(2)}) collective-permute-start(bf16[3,128,256]{2,1,0:T(8,128)(2,1)S(1)} %convert_element_type.3.own), channel_id=1, source_target_pairs={{0,16},{1,65},{2,18},{3,67},{4,20},{5,69},{6,22},{7,71},{8,24},{9,... | collective-permute-start | bytes 589832 | tf_op jit(solution)/shard_map/ppermute | solution.py:30
  36.5 8.4 %collective-permute-start.1 = (bf16[3,128,256]{2,1,0:T(8,128)(2,1)S(1)}, bf16[3,128,256]{2,1,0:T(8,128)(2,1)S(1)}, u32[]{:S(2)}, u32[]{:S(2)}) collective-permute-start(bf16[3,128,256]{2,1,0:T(8,128)(2,1)S(1)} %convert_element_type.3.own), channel_id=1, source_target_pairs={{0,8},{1,33},{2,10},{3,35},{4,12},{5,37},{6,14},{7,39},{8,16},{9,4... | collective-permute-start | bytes 589832 | tf_op jit(solution)/shard_map/ppermute | solution.py:30
  40.3 24.1 %copy-start.1 = (bf16[16,3,128,128]{3,2,1,0:T(8,128)(2,1)}, bf16[16,3,128,128]{3,2,1,0:T(8,128)(2,1)S(1)}, u32[]{:S(2)}) copy-start(bf16[16,3,128,128]{3,2,1,0:T(8,128)(2,1)S(1)} %collective-permute-done.mate.refs_7_) | copy-start | bytes 4718596
  45.7 43.6 %copy-start.2 = (bf16[4,3,128,256]{3,2,1,0:T(8,128)(2,1)}, bf16[4,3,128,256]{3,2,1,0:T(8,128)(2,1)S(1)}, u32[]{:S(2)}) copy-start(bf16[4,3,128,256]{3,2,1,0:T(8,128)(2,1)S(1)} %get-tuple-element.23.refs_8_) | copy-start | bytes 2359300
  45.7 19.3 %collective-permute-start.6 = (bf16[4,3,128,256]{3,2,1,0:T(8,128)(2,1)S(1)}, bf16[4,3,128,256]{3,2,1,0:T(8,128)(2,1)S(1)}, u32[]{:S(2)}, u32[]{:S(2)}) collective-permute-start(bf16[4,3,128,256]{3,2,1,0:T(8,128)(2,1)S(1)} %get-tuple-element.23.refs_8_), channel_id=1, source_target_pairs={{0,96},{1,25},{2,98},{3,27},{4,100},{5,29},{6,102},{7,31},{8,104},... | collective-permute-start | bytes 2359304 | tf_op jit(solution)/shard_map/ppermute | solution.py:30
  46.9 18.3 %collective-permute-start.4 = (bf16[4,3,128,256]{3,2,1,0:T(8,128)(2,1)S(1)}, bf16[4,3,128,256]{3,2,1,0:T(8,128)(2,1)S(1)}, u32[]{:S(2)}, u32[]{:S(2)}) collective-permute-start(bf16[4,3,128,256]{3,2,1,0:T(8,128)(2,1)S(1)} %get-tuple-element.23.refs_8_), channel_id=1, source_target_pairs={{0,32},{1,9},{2,34},{3,11},{4,36},{5,13},{6,38},{7,15},{8,40},{9,1... | collective-permute-start | bytes 2359304 | tf_op jit(solution)/shard_map/ppermute | solution.py:30
  65.0 24.3 %copy-start.3 = (bf16[4,3,128,256]{3,2,1,0:T(8,128)(2,1)}, bf16[4,3,128,256]{3,2,1,0:T(8,128)(2,1)S(1)}, u32[]{:S(2)}) copy-start(bf16[4,3,128,256]{3,2,1,0:T(8,128)(2,1)S(1)} %collective-permute-done.6.refs_10_) | copy-start | bytes 2359300
  65.1 24.3 %collective-permute-start.7 = (bf16[2,3,128,256]{3,2,1,0:T(8,128)(2,1)S(1)}, bf16[2,3,128,256]{3,2,1,0:T(8,128)(2,1)S(1)}, u32[]{:S(2)}, u32[]{:S(2)}) collective-permute-start(bf16[2,3,128,256]{3,2,1,0:T(8,128)(2,1)S(1)} %slice.7), channel_id=1, source_target_pairs={{0,96},{1,25},{2,98},{3,27},{4,100},{5,29},{6,102},{7,31},{8,104},... | collective-permute-start | bytes 1179656 | tf_op jit(solution)/shard_map/ppermute | solution.py:30
  65.2 24.2 %copy-start.4 = (bf16[4,3,128,256]{3,2,1,0:T(8,128)(2,1)}, bf16[4,3,128,256]{3,2,1,0:T(8,128)(2,1)S(1)}, u32[]{:S(2)}) copy-start(bf16[4,3,128,256]{3,2,1,0:T(8,128)(2,1)S(1)} %collective-permute-done.4.refs_9_) | copy-start | bytes 2359300
  65.2 24.1 %collective-permute-start.5 = (bf16[2,3,128,256]{3,2,1,0:T(8,128)(2,1)S(1)}, bf16[2,3,128,256]{3,2,1,0:T(8,128)(2,1)S(1)}, u32[]{:S(2)}, u32[]{:S(2)}) collective-permute-start(bf16[2,3,128,256]{3,2,1,0:T(8,128)(2,1)S(1)} %slice.6), channel_id=1, source_target_pairs={{0,32},{1,9},{2,34},{3,11},{4,36},{5,13},{6,38},{7,15},{8,40},{9,1... | collective-permute-start | bytes 1179656 | tf_op jit(solution)/shard_map/ppermute | solution.py:30

commit v5 on v4

--- a/solution.py
+++ b/solution.py
@@ -178,13 +178,17 @@
     squares[...] = jnp.broadcast_to(jnp.sum(acc, axis=(0, 1), keepdims=True).reshape(1, 1, 1), squares.shape)
 
 
-def stack_kernel(own, near_back, opposite, near_front, moments, line, held, raw, sem):
-    load = pltpu.make_async_copy(moments, raw, sem)
+def hold_kernel(moments, held):
+    held[...] = 0.8 * moments[...]
+
+
+def stack_kernel(own, near_back, opposite, near_front, held, line, kept, raw, sem):
+    load = pltpu.make_async_copy(held, raw, sem)
     load.start()
     for i, block in enumerate((own, near_back, opposite, near_front)):
         line[i] = block[...]
     load.wait()
-    held[...] = 0.8 * raw[...]
+    kept[...] = raw[...]
 
 
 def update_kernel(entries, squares, gathered, far_first, far_last, factors, master, mine, mate, *refs):
@@ -286,11 +290,12 @@
     mine = exchange(spread, FS)
 
     own = master_weights.astype(BF)
-    near_back = turn(own, True, 1)
-    near_front = turn(own, True, -1)
-    opposite = turn(own, True, 2)
-
     grads = gradients(normed_input, output_cotangent, query_grad, key_grad, attn_values)
+    late = after(own, grads)
+    near_back = turn(late, True, 1)
+    near_front = turn(late, True, -1)
+    opposite = turn(late, True, 2)
+    (held,) = call(hold_kernel, [jax.ShapeDtypeStruct((3, 16, 256), F32)], [moments])
     mine = after(mine, grads)
     mate = swap(mine)
     kept, part = call(
@@ -309,7 +314,7 @@
     line, held = call(
         stack_kernel,
         [jax.ShapeDtypeStruct((4, 3, 128, 256), BF), jax.ShapeDtypeStruct((3, 16, 256), F32)],
-        [after(own, parts), near_back, opposite, near_front] + held_in_hbm([moments]),
+        [after(own, parts), near_back, opposite, near_front] + held_in_hbm([held]),
         [pltpu.VMEM((3, 16, 256), F32), pltpu.SemaphoreType.DMA],
         ins=vmem(4) + hbm(1),
     )

time: 95.2 us -> 95.2 us (level)
    pallas_call x8 -> x9, Pallas kernels: 24.4 us -> 24.4 us  [call(): pl.pallas_call(kernel, out_shape=outs, in_specs=ins or vmem(len(args)), o...]
where the time goes in v5:
time: 95.2 us; the launch traced here: 94.1 us
  blocking collectives  38.4 us (40%)
  Pallas kernels  24.4 us (26%)
  waiting for transfers between devices  16 us (17%)
  starting transfers between devices  14.4 us (15%)
    all_to_all x3, blocking collectives, exchange(): return lax.all_to_all(value, axes, 0, 0, tiled=True)  38.4 us
    pallas_call x9, Pallas kernels, call(): pl.pallas_call(kernel, out_shape=outs, in_specs=ins or vmem(len(args)), o...  24.4 us
    all_to_all x1, waiting for transfers between devices, exchange(): return lax.all_to_all(value, axes, 0, 0, tiled=True)  12.5 us
    all_to_all x1, starting transfers between devices, exchange(): return lax.all_to_all(value, axes, 0, 0, tiled=True)  8 us
    ppermute x7, starting transfers between devices, turn(): return lax.ppermute(value, FS + TP, pairs)  6.35 us
    ppermute x7, waiting for transfers between devices, turn(): return lax.ppermute(value, FS + TP, pairs)  3.47 us
  transfers between devices with their start and end apart: 9, of which 3 were waited for; matrix products, arithmetic and copies ran while one was open for 0% of the time, Pallas kernels for 18%

profile of v5, /device:TPU:0, one launch (start us, length us, event | category | flops | bytes accessed | tf_op | source)
XLA Modules:
  0.0 94.1 jit_solution(1295183539536153477)
XLA Ops:
  0.6 2.2 %shard_map.111 = bf16[16,3,128,128]{3,2,1,0:T(8,128)(2,1)} custom-call(bf16[3,128,256]{2,1,0:T(8,128)(2,1)} %refs_4_.1), custom_call_target="tpu_custom_call" | custom-call | tf_op jit(solution)/shard_map/pallas_call | solution.py:46
  2.9 8.0 %all-to-all-start = ((bf16[16,3,128,128]{3,2,1,0:T(8,128)(2,1)}), bf16[16,3,128,128]{3,2,1,0:T(8,128)(2,1)S(1)}, u32[]{:S(2)}, u32[]{:S(2)}) async-start(bf16[16,3,128,128]{3,2,1,0:T(8,128)(2,1)} %shard_map.111), calls=%async_computation | async-start | bytes 3145728 | tf_op jit(solution)/shard_map/all_to_all | solution.py:34
  10.9 0.0 copy-start.7
  10.9 0.0 copy-start.4
  10.9 12.0 %shard_map.112.grads = bf16[3,256,2048]{2,1,0:T(8,128)(2,1)} custom-call(bf16[2048,2048]{1,0:T(8,128)(2,1)} %first.1, bf16[2048,2048]{1,0:T(8,128)(2,1)} %second.1, bf16[2048,256]{1,0:T(8,128)(2,1)} %q.1, bf16[2048,256]{1,0:T(8,128)(2,1)} %k.1, bf16[2048,256]{1,0:T(8,128)(2,1)} %v.1), custom_call_target="tpu_custom_call" | custom-call | tf_op jit(solution)/shard_map/pallas_call | solution.py:46
  22.9 12.5 %all-to-all-done.mine.refs_6_ = bf16[16,3,128,128]{3,2,1,0:T(8,128)(2,1)S(1)} async-done(((bf16[16,3,128,128]{3,2,1,0:T(8,128)(2,1)}), bf16[16,3,128,128]{3,2,1,0:T(8,128)(2,1)S(1)}, u32[]{:S(2)}, u32[]{:S(2)}) %all-to-all-start) | async-done | bytes 1572896 | tf_op jit(solution)/shard_map/all_to_all | solution.py:34
  35.4 0.0 copy-start
  35.4 0.0 collective-permute-start
  35.4 0.0 copy-done.7
  35.4 0.1 collective-permute-start.3
  35.5 1.0 %collective-permute-start.2 = (bf16[3,128,256]{2,1,0:T(8,128)(2,1)S(1)}, bf16[3,128,256]{2,1,0:T(8,128)(2,1)S(1)}, u32[]{:S(2)}, u32[]{:S(2)}) collective-permute-start(bf16[3,128,256]{2,1,0:T(8,128)(2,1)S(1)} %convert_element_type.3.own), channel_id=1, source_target_pairs={{0,16},{1,65},{2,18},{3,67},{4,20},{5,69},{6,22},{7,71},{8,24},{9,... | collective-permute-start | bytes 589832 | tf_op jit(solution)/shard_map/ppermute | solution.py:30
  36.5 1.1 %collective-permute-start.1 = (bf16[3,128,256]{2,1,0:T(8,128)(2,1)S(1)}, bf16[3,128,256]{2,1,0:T(8,128)(2,1)S(1)}, u32[]{:S(2)}, u32[]{:S(2)}) collective-permute-start(bf16[3,128,256]{2,1,0:T(8,128)(2,1)S(1)} %convert_element_type.3.own), channel_id=1, source_target_pairs={{0,8},{1,33},{2,10},{3,35},{4,12},{5,37},{6,14},{7,39},{8,16},{9,4... | collective-permute-start | bytes 589832 | tf_op jit(solution)/shard_map/ppermute | solution.py:30
  37.5 0.0 copy-done.4
  37.5 0.0 copy-start.3
  37.6 2.8 %shard_map.113 = (bf16[3,256,2048]{2,1,0:T(8,128)(2,1)S(1)}, bf16[3,128,256]{2,1,0:T(8,128)(2,1)S(1)}) custom-call(bf16[16,3,128,128]{3,2,1,0:T(8,128)(2,1)S(1)} %all-to-all-done.mine.refs_6_, bf16[3,256,2048]{2,1,0:T(8,128)(2,1)} %shard_map.112.grads), custom_call_target="tpu_custom_call" | custom-call | tf_op jit(solution)/shard_map/pallas_call | solution.py:46
  40.3 0.0 collective-permute-done.mate.refs_7_
  40.3 0.0 copy-start.1
  40.3 1.0 %shard_map.114 = bf16[16,3,16,256]{3,2,1,0:T(8,128)(2,1)S(1)} custom-call(bf16[16,3,128,128]{3,2,1,0:T(8,128)(2,1)S(1)} %collective-permute-done.mate.refs_7_, bf16[3,256,2048]{2,1,0:T(8,128)(2,1)S(1)} %get-tuple-element.19.grads, bf16[3,128,256]{2,1,0:T(8,128)(2,1)S(1)} %get-tuple-element.20.part), custom_call_target="tpu_custom_call" | custom-call | tf_op jit(solution)/shard_map/pallas_call | solution.py:46
  41.4 0.0 copy-done
  41.4 0.0 copy-done.3
  41.4 0.0 collective-permute-done.3.near_front
  41.4 1.4 %collective-permute-done.2.opposite = bf16[3,128,256]{2,1,0:T(8,128)(2,1)S(1)} collective-permute-done((bf16[3,128,256]{2,1,0:T(8,128)(2,1)S(1)}, bf16[3,128,256]{2,1,0:T(8,128)(2,1)S(1)}, u32[]{:S(2)}, u32[]{:S(2)}) %collective-permute-start.2) | collective-permute-done | bytes 196640 | tf_op jit(solution)/shard_map/ppermute | solution.py:30
  42.9 2.0 %collective-permute-done.1.near_back = bf16[3,128,256]{2,1,0:T(8,128)(2,1)S(1)} collective-permute-done((bf16[3,128,256]{2,1,0:T(8,128)(2,1)S(1)}, bf16[3,128,256]{2,1,0:T(8,128)(2,1)S(1)}, u32[]{:S(2)}, u32[]{:S(2)}) %collective-permute-start.1) | collective-permute-done | bytes 196640 | tf_op jit(solution)/shard_map/ppermute | solution.py:30
  44.9 0.8 shard_map.116
  45.7 0.0 copy-start.2
  45.7 1.2 %collective-permute-start.6 = (bf16[4,3,128,256]{3,2,1,0:T(8,128)(2,1)S(1)}, bf16[4,3,128,256]{3,2,1,0:T(8,128)(2,1)S(1)}, u32[]{:S(2)}, u32[]{:S(2)}) collective-permute-start(bf16[4,3,128,256]{3,2,1,0:T(8,128)(2,1)S(1)} %get-tuple-element.25.refs_8_), channel_id=1, source_target_pairs={{0,96},{1,25},{2,98},{3,27},{4,100},{5,29},{6,102},{7,31},{8,104},... | collective-permute-start | bytes 2359304 | tf_op jit(solution)/shard_map/ppermute | solution.py:30
  46.9 0.9 collective-permute-start.4
  47.8 16.5 %all_to_all.20.parts = bf16[16,3,16,256]{3,2,1,0:T(8,128)(2,1)S(1)} all-to-all(bf16[16,3,16,256]{3,2,1,0:T(8,128)(2,1)S(1)} %shard_map.114), channel_id=1, replica_groups=mesh['fs_0'=4,'fs_1'=4,'tp_0'=4,'tp_1'=2] {'fs_0','fs_1'}, dimensions={0} | all-to-all | bytes 786432 | tf_op jit(solution)/shard_map/all_to_all | solution.py:34
  64.3 0.0 copy-done.1
  64.3 0.7 shard_map.117
  65.0 0.0 collective-permute-done.6.refs_10_
  65.0 0.0 copy-start.5
  65.1 0.1 collective-permute-start.7
  65.2 0.0 collective-permute-done.4.refs_9_
  65.2 0.0 copy-start.6
  65.2 2.0 %collective-permute-start.5 = (bf16[2,3,128,256]{3,2,1,0:T(8,128)(2,1)S(1)}, bf16[2,3,128,256]{3,2,1,0:T(8,128)(2,1)S(1)}, u32[]{:S(2)}, u32[]{:S(2)}) collective-permute-start(bf16[2,3,128,256]{3,2,1,0:T(8,128)(2,1)S(1)} %slice.6), channel_id=1, source_target_pairs={{0,32},{1,9},{2,34},{3,11},{4,36},{5,13},{6,38},{7,15},{8,40},{9,1... | collective-permute-start | bytes 1179656 | tf_op jit(solution)/shard_map/ppermute | solution.py:30
  67.3 12.3 %all_to_all.21.gathered.refs_1_ = bf16[16,3,16,256]{3,2,1,0:T(8,128)(2,1)S(1)} all-to-all(bf16[16,3,16,256]{3,2,1,0:T(8,128)(2,1)S(1)} %get-tuple-element.24), channel_id=1, replica_groups=mesh['fs_0'=4,'fs_1'=4,'tp_0'=4,'tp_1'=2] {'fs_0','fs_1'}, dimensions={0} | all-to-all | bytes 786432 | tf_op jit(solution)/shard_map/all_to_all | solution.py:34
  79.6 0.1 shard_map.118
  79.8 9.6 %all_to_all.22.refs_0_ = f32[8,1,128]{2,1,0:T(1,128)S(1)} all-to-all(f32[8,1,128]{2,1,0:T(1,128)S(1)} %shard_map.118), channel_id=1, replica_groups=mesh['fs_0'=4,'fs_1'=4,'tp_0'=4,'tp_1'=2] {'tp_0','tp_1'}, dimensions={0} | all-to-all | bytes 8192 | tf_op jit(solution)/shard_map/all_to_all | solution.py:34
  89.3 0.0 collective-permute-done.7.refs_3_
  89.3 0.0 collective-permute-done.5.refs_2_
  89.3 0.0 copy-done.2
  89.3 0.0 copy-done.5
  89.3 0.0 copy-done.6
  89.3 4.8 %shard_map.119 = (f32[3,128,256]{2,1,0:T(8,128)}, f32[3,128,256]{2,1,0:T(8,128)}, bf16[3,2048,256]{2,1,0:T(8,128)(2,1)}) custom-call(f32[8,1,128]{2,1,0:T(1,128)S(1)} %all_to_all.22.refs_0_, bf16[16,3,16,256]{3,2,1,0:T(8,128)(2,1)S(1)} %all_to_all.21.gathered.refs_1_, bf16[2,3,128,256]{3,2,1,0:T(8,128)(2,1)S(1)} %collective-permute-done.5.refs_2_, ...), custom_call_target="tpu_custom_call" | custom-call | tf_op jit(solution)/shard_map/pallas_call | solution.py:46
  (4 shorter events, 0.1 us)
Async XLA Ops:
  2.9 32.5 %all-to-all-start = ((bf16[16,3,128,128]{3,2,1,0:T(8,128)(2,1)}), bf16[16,3,128,128]{3,2,1,0:T(8,128)(2,1)S(1)}, u32[]{:S(2)}, u32[]{:S(2)}) async-start(bf16[16,3,128,128]{3,2,1,0:T(8,128)(2,1)} %shard_map.111), calls=%async_computation | async-start | bytes 3145728 | tf_op jit(solution)/shard_map/all_to_all | solution.py:34
  10.9 24.5 %copy-start.7 = (f32[3,128,256]{2,1,0:T(8,128)S(1)}, f32[3,128,256]{2,1,0:T(8,128)}, u32[]{:S(2)}) copy-start(f32[3,128,256]{2,1,0:T(8,128)} %refs_5_.1) | copy-start | bytes 1179652
  10.9 26.7 %copy-start.4 = (f32[3,16,256]{2,1,0:T(8,128)S(1)}, f32[3,16,256]{2,1,0:T(8,128)}, u32[]{:S(2)}) copy-start(f32[3,16,256]{2,1,0:T(8,128)} %moments.1) | copy-start | bytes 147460
  35.4 6.0 %copy-start = (bf16[16,3,128,128]{3,2,1,0:T(8,128)(2,1)}, bf16[16,3,128,128]{3,2,1,0:T(8,128)(2,1)S(1)}, u32[]{:S(2)}) copy-start(bf16[16,3,128,128]{3,2,1,0:T(8,128)(2,1)S(1)} %all-to-all-done.mine.refs_6_) | copy-start | bytes 4718596
  35.4 4.9 %collective-permute-start = (bf16[16,3,128,128]{3,2,1,0:T(8,128)(2,1)S(1)}, bf16[16,3,128,128]{3,2,1,0:T(8,128)(2,1)S(1)}, u32[]{:S(2)}, u32[]{:S(2)}) collective-permute-start(bf16[16,3,128,128]{3,2,1,0:T(8,128)(2,1)S(1)} %all-to-all-done.mine.refs_6_), channel_id=1, source_target_pairs={{0,1},{1,0},{2,3},{3,2},{4,5},{5,4},{6,7},{7,6},{8,9},{9,8},{10,11... | collective-permute-start | bytes 4718600 | tf_op jit(solution)/shard_map/ppermute | solution.py:18
  35.4 6.0 %collective-permute-start.3 = (bf16[3,128,256]{2,1,0:T(8,128)(2,1)S(1)}, bf16[3,128,256]{2,1,0:T(8,128)(2,1)S(1)}, u32[]{:S(2)}, u32[]{:S(2)}) collective-permute-start(bf16[3,128,256]{2,1,0:T(8,128)(2,1)S(1)} %convert_element_type.3.own), channel_id=1, source_target_pairs={{0,24},{1,97},{2,26},{3,99},{4,28},{5,101},{6,30},{7,103},{8,0},{9... | collective-permute-start | bytes 589832 | tf_op jit(solution)/shard_map/ppermute | solution.py:30
  35.5 7.4 %collective-permute-start.2 = (bf16[3,128,256]{2,1,0:T(8,128)(2,1)S(1)}, bf16[3,128,256]{2,1,0:T(8,128)(2,1)S(1)}, u32[]{:S(2)}, u32[]{:S(2)}) collective-permute-start(bf16[3,128,256]{2,1,0:T(8,128)(2,1)S(1)} %convert_element_type.3.own), channel_id=1, source_target_pairs={{0,16},{1,65},{2,18},{3,67},{4,20},{5,69},{6,22},{7,71},{8,24},{9,... | collective-permute-start | bytes 589832 | tf_op jit(solution)/shard_map/ppermute | solution.py:30
  36.5 8.4 %collective-permute-start.1 = (bf16[3,128,256]{2,1,0:T(8,128)(2,1)S(1)}, bf16[3,128,256]{2,1,0:T(8,128)(2,1)S(1)}, u32[]{:S(2)}, u32[]{:S(2)}) collective-permute-start(bf16[3,128,256]{2,1,0:T(8,128)(2,1)S(1)} %convert_element_type.3.own), channel_id=1, source_target_pairs={{0,8},{1,33},{2,10},{3,35},{4,12},{5,37},{6,14},{7,39},{8,16},{9,4... | collective-permute-start | bytes 589832 | tf_op jit(solution)/shard_map/ppermute | solution.py:30
  37.5 3.9 %copy-start.3 = (f32[3,16,256]{2,1,0:T(8,128)}, f32[3,16,256]{2,1,0:T(8,128)S(1)}, u32[]{:S(2)}) copy-start(f32[3,16,256]{2,1,0:T(8,128)S(1)} %shard_map.115.held) | copy-start | bytes 147460
  40.3 24.0 %copy-start.1 = (bf16[16,3,128,128]{3,2,1,0:T(8,128)(2,1)}, bf16[16,3,128,128]{3,2,1,0:T(8,128)(2,1)S(1)}, u32[]{:S(2)}) copy-start(bf16[16,3,128,128]{3,2,1,0:T(8,128)(2,1)S(1)} %collective-permute-done.mate.refs_7_) | copy-start | bytes 4718596
  45.7 43.6 %copy-start.2 = (bf16[4,3,128,256]{3,2,1,0:T(8,128)(2,1)}, bf16[4,3,128,256]{3,2,1,0:T(8,128)(2,1)S(1)}, u32[]{:S(2)}) copy-start(bf16[4,3,128,256]{3,2,1,0:T(8,128)(2,1)S(1)} %get-tuple-element.25.refs_8_) | copy-start | bytes 2359300
  45.7 19.3 %collective-permute-start.6 = (bf16[4,3,128,256]{3,2,1,0:T(8,128)(2,1)S(1)}, bf16[4,3,128,256]{3,2,1,0:T(8,128)(2,1)S(1)}, u32[]{:S(2)}, u32[]{:S(2)}) collective-permute-start(bf16[4,3,128,256]{3,2,1,0:T(8,128)(2,1)S(1)} %get-tuple-element.25.refs_8_), channel_id=1, source_target_pairs={{0,96},{1,25},{2,98},{3,27},{4,100},{5,29},{6,102},{7,31},{8,104},... | collective-permute-start | bytes 2359304 | tf_op jit(solution)/shard_map/ppermute | solution.py:30
  46.9 18.3 %collective-permute-start.4 = (bf16[4,3,128,256]{3,2,1,0:T(8,128)(2,1)S(1)}, bf16[4,3,128,256]{3,2,1,0:T(8,128)(2,1)S(1)}, u32[]{:S(2)}, u32[]{:S(2)}) collective-permute-start(bf16[4,3,128,256]{3,2,1,0:T(8,128)(2,1)S(1)} %get-tuple-element.25.refs_8_), channel_id=1, source_target_pairs={{0,32},{1,9},{2,34},{3,11},{4,36},{5,13},{6,38},{7,15},{8,40},{9,1... | collective-permute-start | bytes 2359304 | tf_op jit(solution)/shard_map/ppermute | solution.py:30
  65.0 24.3 %copy-start.5 = (bf16[4,3,128,256]{3,2,1,0:T(8,128)(2,1)}, bf16[4,3,128,256]{3,2,1,0:T(8,128)(2,1)S(1)}, u32[]{:S(2)}) copy-start(bf16[4,3,128,256]{3,2,1,0:T(8,128)(2,1)S(1)} %collective-permute-done.6.refs_10_) | copy-start | bytes 2359300
  65.1 24.3 %collective-permute-start.7 = (bf16[2,3,128,256]{3,2,1,0:T(8,128)(2,1)S(1)}, bf16[2,3,128,256]{3,2,1,0:T(8,128)(2,1)S(1)}, u32[]{:S(2)}, u32[]{:S(2)}) collective-permute-start(bf16[2,3,128,256]{3,2,1,0:T(8,128)(2,1)S(1)} %slice.7), channel_id=1, source_target_pairs={{0,96},{1,25},{2,98},{3,27},{4,100},{5,29},{6,102},{7,31},{8,104},... | collective-permute-start | bytes 1179656 | tf_op jit(solution)/shard_map/ppermute | solution.py:30
  65.2 24.2 %copy-start.6 = (bf16[4,3,128,256]{3,2,1,0:T(8,128)(2,1)}, bf16[4,3,128,256]{3,2,1,0:T(8,128)(2,1)S(1)}, u32[]{:S(2)}) copy-start(bf16[4,3,128,256]{3,2,1,0:T(8,128)(2,1)S(1)} %collective-permute-done.4.refs_9_) | copy-start | bytes 2359300
  65.2 24.1 %collective-permute-start.5 = (bf16[2,3,128,256]{3,2,1,0:T(8,128)(2,1)S(1)}, bf16[2,3,128,256]{3,2,1,0:T(8,128)(2,1)S(1)}, u32[]{:S(2)}, u32[]{:S(2)}) collective-permute-start(bf16[2,3,128,256]{3,2,1,0:T(8,128)(2,1)S(1)} %slice.6), channel_id=1, source_target_pairs={{0,32},{1,9},{2,34},{3,11},{4,36},{5,13},{6,38},{7,15},{8,40},{9,1... | collective-permute-start | bytes 1179656 | tf_op jit(solution)/shard_map/ppermute | solution.py:30
